TPU v7x, 128 devices: a whole 4x4x4 slice. The times are simulated.
128 devices in a mesh: sp: 16 (over z, x), tp: 8 (over y, core).
Axes of the slice: x: 4, y: 4, z: 4, core: 2. Of those that a mesh axis runs over, the one named last changes fastest.
Arguments:
- queries: bfloat16 [8192, 2048], P('sp', 'tp'), may hold values from -6 to 6
- keys: bfloat16 [8192, 1024], P('sp', 'tp'), may hold values from -6 to 6
- values: bfloat16 [8192, 1024], P('sp', 'tp'), may hold values from -6 to 6
- documents: int32 [8192], P('sp'), may hold values from 0 to 3, never falling along the last dimension, each value on 1 to 4096 neighbouring positions
- query_gain: float32 [128], replicated, may hold values from 1.8 to 6
- key_gain: float32 [128], replicated, may hold values from 1.8 to 6
- residual: bfloat16 [8192, 4096], P('sp', 'tp'), may hold values from -6 to 6
- out_weight: bfloat16 [2048, 4096], P('tp'), may hold values from -0.125 to 0.125
- norm_gain: float32 [4096], replicated, may hold values from 0.1 to 1.9
- up_weight: bfloat16 [4096, 16384], P('sp', 'tp'), may hold values from -0.09375 to 0.09375
- down_weight: bfloat16 [16384, 4096], P('tp', 'sp'), may hold values from -0.046875 to 0.046875
Outputs:
- mixed: bfloat16 [8192, 4096], P('sp', 'tp')
Inputs may be any that keep to these rules, and one draw needn't show every extreme that they name: `documents`: document numbers never fall along the sequence; a document has at most 4096 positions.
All inputs are finite; a program needn't handle non-finite values.
Results may differ from a plain program's by a relative error of at most 0.017.
The roundings to bfloat16 on the way count: a program that leaves them out, or rounds other values in their place, can miss the bound.
Values may be sent and summed in bfloat16 or wider, within the bound.
A program may use at most 192 MiB of HBM per device.

v0:
```python
import jax
import jax.numpy as jnp
from jax import lax
from jax.sharding import Mesh
from jax.sharding import PartitionSpec as P

D = 4096
HQ = 16
KV = 8
HD = 128
GRID_W = 64
TP = ("tp_0", "tp_1")


norm_eps = 1e-06
rope_base = 10000.0
masked_score = -1e30


def gather_turned(arrays, axis, dims):
    turned = [jnp.moveaxis(a, dim, 0) for a, dim in zip(arrays, dims)]
    both = jnp.concatenate([t.reshape(len(t), -1) for t in turned], axis=1)
    filled, at, finished = (lax.all_gather(both, axis, axis=0, tiled=True), 0, [])
    for t, dim in zip(turned, dims):
        section = filled[:, at : at + t[0].size].reshape(-1, *t.shape[1:])
        finished.append(jnp.moveaxis(section, 0, dim))
        at += t[0].size
    return tuple(finished)


def in_one_piece(arrays, axis, dim, along):
    columns = [a.reshape(*a.shape[:along], -1) for a in arrays]
    both = jnp.concatenate(columns, axis=along)
    filled, at, finished = (lax.all_gather(both, axis, axis=dim, tiled=True), 0, [])
    for a, column in zip(arrays, columns):
        section = filled[..., at : at + column.shape[along]]
        finished.append(section.reshape(*section.shape[:along], *a.shape[along:]))
        at += column.shape[along]
    return tuple(finished)


def split_up(x, dim, size):
    dims = x.shape
    pieces = x.reshape(*dims[:dim], size, dims[dim] // size, *dims[dim + 1 :])
    return jnp.moveaxis(pieces, dim, 0)


def sum_at_owner(x, axis, dim):
    pieces = split_up(x, dim, lax.axis_size(axis))
    arrived = lax.all_to_all(pieces, axis, split_axis=0, concat_axis=0, tiled=True)
    return arrived.astype(jnp.float32).sum(axis=0)


def sent_to_all(x, axis):
    copies = jnp.broadcast_to(x, (lax.axis_size(axis), *x.shape))
    return lax.all_to_all(copies, axis, split_axis=0, concat_axis=0, tiled=True)


def over_copies(x, axis):
    return sent_to_all(x, axis).sum(axis=0)


def joined_along(pieces, dim):
    pieces = jnp.moveaxis(pieces, 0, dim)
    dims = pieces.shape
    return pieces.reshape(*dims[:dim], dims[dim] * dims[dim + 1], *dims[dim + 2 :])


def whole_of(x, axes, dim):
    far, near = axes
    initial = sent_to_all(x, far)
    pieces = jnp.swapaxes(sent_to_all(initial, near), 0, 1)
    return joined_along(pieces.reshape(-1, *x.shape), dim)


def head_norm(heads_in, gain):
    values32 = heads_in.astype(jnp.float32)
    scaled = values32 * lax.rsqrt(jnp.mean(values32 * values32, axis=-1, keepdims=True) + norm_eps)
    return scaled * gain


def rotate_half(heads_in, position):
    quarter = heads_in.shape[-1] // 2
    inverse_freq = rope_base ** (-jnp.arange(quarter, dtype=jnp.float32) / quarter)
    angles = position[:, None] * inverse_freq[None, :]
    cosine_part = jnp.cos(angles)[:, None, :]
    sine_part = jnp.sin(angles)[:, None, :]
    leading = heads_in[..., :quarter]
    trailing = heads_in[..., quarter:]
    return jnp.concatenate(
        [
            leading * cosine_part - trailing * sine_part,
            leading * sine_part + trailing * cosine_part,
        ],
        axis=-1,
    )


def grid_rotary(heads_in, positions):
    half_width = heads_in.shape[-1] // 2
    grid_row = (positions // GRID_W).astype(jnp.float32)
    grid_col = (positions % GRID_W).astype(jnp.float32)
    return jnp.concatenate(
        [
            rotate_half(heads_in[..., :half_width], grid_row),
            rotate_half(heads_in[..., half_width:], grid_col),
        ],
        axis=-1,
    )


def body(
    queries,
    keys,
    values,
    documents,
    query_gain,
    key_gain,
    residual,
    out_weight,
    norm_gain,
    up_weight,
    down_weight,
):
    tok_rows = queries.shape[0]
    key_heads = keys.shape[1] // HD
    group_size = HQ // KV
    width_local = residual.shape[1]
    tp_index = lax.axis_index(TP)
    up_whole, down_whole = gather_turned((up_weight, down_weight), "sp", (0, 1))
    positions = lax.axis_index("sp") * tok_rows + jnp.arange(tok_rows, dtype=jnp.int32)
    queries_rot = grid_rotary(
        head_norm(queries.reshape(tok_rows, key_heads * group_size, HD), query_gain), positions
    )
    queries_rot = queries_rot.astype(jnp.bfloat16).reshape(tok_rows, key_heads, group_size, HD)
    keys_rot = grid_rotary(
        head_norm(keys.reshape(tok_rows, key_heads, HD), key_gain), positions
    ).astype(jnp.bfloat16)
    value_heads = values.reshape(tok_rows, key_heads, HD)
    own_docs = documents.astype(jnp.bfloat16)
    score_scale = HD ** (-0.5)
    running_max = jnp.full((key_heads, group_size, tok_rows), masked_score, jnp.float32)
    key_piece, value_piece, doc_piece = in_one_piece((keys_rot, value_heads, own_docs), "sp", 0, 1)
    scores = (
        jnp.einsum("qkgd,skd->kgqs", queries_rot, key_piece, preferred_element_type=jnp.float32)
        * score_scale
    )
    same_doc = own_docs[:, None] == doc_piece[None, :]
    scores = jnp.where(same_doc, scores, masked_score)
    new_max = jnp.maximum(running_max, jnp.max(scores, axis=-1))
    probs = jnp.where(same_doc, jnp.exp(scores - new_max[..., None]), 0.0)
    running_sum = jnp.sum(probs, axis=-1)
    update = jnp.einsum(
        "kgqs,skd->qkgd",
        probs.astype(jnp.bfloat16),
        value_piece,
        preferred_element_type=jnp.float32,
    )
    weighted = update
    running_max, running_sum, weighted = (new_max, running_sum, weighted)
    attended = (weighted / jnp.transpose(running_sum, (2, 0, 1))[..., None]).astype(jnp.bfloat16)
    attended = attended.reshape(tok_rows, key_heads * group_size * HD)
    partial_out = jnp.dot(attended, out_weight, preferred_element_type=jnp.float32)
    branch = sum_at_owner(partial_out.astype(jnp.bfloat16), TP, 1)
    stream = residual.astype(jnp.float32) + branch
    square_sum = over_copies(jnp.sum(stream * stream, axis=-1), TP)
    gain_local = lax.dynamic_slice_in_dim(norm_gain, tp_index * width_local, width_local, 0)
    normed_local = stream * lax.rsqrt(square_sum[:, None] / D + norm_eps) * gain_local
    normed = whole_of(normed_local.astype(jnp.bfloat16), ("tp_0", "tp_1"), 1)
    hidden = jnp.dot(normed, up_whole, preferred_element_type=jnp.float32)
    positive = jnp.maximum(hidden, 0.0)
    squared = (positive * positive).astype(jnp.bfloat16)
    product = jnp.dot(squared, down_whole, preferred_element_type=jnp.float32)
    feed = lax.psum_scatter(
        product.astype(jnp.bfloat16), TP, scatter_dimension=1, tiled=True
    ).astype(jnp.float32)
    return (stream + feed).astype(jnp.bfloat16)


def solution(mesh):
    split = Mesh(mesh.devices.reshape(mesh.shape["sp"], 4, 2), ("sp", "tp_0", "tp_1"))
    return jax.shard_map(
        body,
        mesh=split,
        in_specs=(
            P("sp", TP),
            P("sp", TP),
            P("sp", TP),
            P("sp"),
            P(),
            P(),
            P("sp", TP),
            P(TP, None),
            P(),
            P("sp", TP),
            P(TP, "sp"),
        ),
        out_specs=P("sp", TP),
        check_vma=False,
    )
```

profile of v0, /device:TPU:0, one launch (start us, length us, event | category | flops | bytes accessed | tf_op | source)
XLA Modules:
  0.0 357.3 jit_solution(17306286537889101392)
XLA Ops:
  6.5 0.0 copy-start
  6.5 0.0 copy-start.3
  6.5 0.0 all-gather.3.cloned.1.call-start
  6.6 1.2 copy.50
  7.8 0.7 fusion.31
  8.6 0.6 fusion.57
  9.1 0.1 copy.51
  9.3 0.1 copy.52
  9.4 0.1 copy.53
  9.5 0.1 copy.54
  9.7 0.7 convert_element_type.70
  10.3 0.1 reshape.364
  10.5 0.0 copy-start.4
  10.5 1.8 concatenate.30
  12.3 0.0 all-gather.3.cloned.1.call-update
  12.4 0.0 all-gather.5.cloned.1.call-start
  12.4 1.5 copy.64
  13.9 2.7 pad_maximum_fusion
  16.6 0.0 all-gather.5.cloned.1.call-update
  16.6 0.0 copy-done.3
  16.6 0.1 copy.56
  16.8 0.1 copy.57
  16.9 0.1 multiply_reduce_fusion.1
  17.0 1.9 multiply_cosine_fusion.1
  18.9 0.0 copy-done.4
  18.9 0.2 multiply_multiply_fusion
  19.1 0.5 subtract_convert_fusion.1
  19.6 56.8 %all-gather.3.cloned.1.call-done = bf16[8192,257]{1,0:T(8,128)(2,1)} async-done(((bf16[512,257]{1,0:T(8,128)(2,1)}), bf16[8192,257]{1,0:T(8,128)(2,1)}) %all-gather.3.cloned.1.call-update) | async-done | bytes 4210704 | tf_op jit(solution)/shard_map/all_gather | solution.py:34
  76.4 2.2 slice_reduce_fusion
  78.7 4.0 %broadcast_compare_fusion = pred[512,8192]{0,1:T(8,128)(4,1)} fusion(bf16[512]{0:T(512)(128)(2,1)S(1)} %convert_element_type.70, bf16[8192]{0:T(1024)(128)(2,1)S(1)} %slice_reduce_fusion), kind=kLoop, calls=%fused_computation.17 | loop fusion | flops 4194304 | bytes 4211712 | tf_op jit(solution)/shard_map/eq | solution.py:148
  82.6 17.1 %fusion = (f32[2,512]{1,0:T(2,128)S(1)}, f32[8192,512,2]{1,0,2:T(8,128)}) fusion(pred[512,8192]{0,1:T(8,128)(4,1)} %broadcast_compare_fusion, bf16[512,2,32]{2,0,1:T(8,128)(2,1)S(1)} %get-tuple-element.9, bf16[512,2,32]{2,0,1:T(8,128)(2,1)S(1)} %get-tuple-element.10, bf16[512,2,32]{2,0,1:T(8,128)(2,1)S(1)} %get-tuple-element.6, ...), kind=kOutput, calls=%fused_computation.2 | convolution fusion | flops 2173697024 | bytes 40112128 | tf_op jit(solution)/shard_map/qkgd,skd->kgqs/dot_general | solution.py:145
  99.7 15.8 %fusion.1 = f32[2,512]{1,0:T(2,128)S(1)} fusion(f32[8192,512,2]{1,0,2:T(8,128)} %get-tuple-element.24, f32[2,512]{1,0:T(2,128)S(1)} %broadcast_maximum_fusion, pred[512,8192]{0,1:T(8,128)(4,1)} %broadcast_compare_fusion), kind=kLoop, calls=%fused_computation.3 | loop fusion | flops 41942016 | bytes 37756928 | tf_op jit(solution)/shard_map/reduce_sum | solution.py:152
  115.6 17.6 %fusion.26 = bf16[512,1,2,128]{0,3,2,1:T(8,128)(2,1)S(1)} fusion(f32[8192,512,2]{1,0,2:T(8,128)} %get-tuple-element.24, f32[2,512]{1,0:T(2,128)S(1)} %broadcast_maximum_fusion, pred[512,8192]{0,1:T(8,128)(4,1)} %broadcast_compare_fusion, bf16[8192,257]{1,0:T(8,128)(2,1)} %all-gather.3.cloned.1.call-done, f32[512,2]{0,1:T(2,128)S(1)} %bitcast.100), kind=kOutput, calls=%fused_computation.30 | convolution fusion | flops 2189688832 | bytes 40116224 | tf_op jit(solution)/shard_map/kgqs,skd->qkgd/dot_general | solution.py:153
  133.1 0.0 copy-done
  133.1 1.3 convolution_convert_fusion
  134.4 0.4 copy.71
  134.8 0.0 copy-start.2
  134.8 53.9 %all_to_all.21 = bf16[8,512,512]{2,1,0:T(8,128)(2,1)S(1)} all-to-all(bf16[8,512,512]{2,1,0:T(8,128)(2,1)S(1)} %bitcast.94), channel_id=1, replica_groups=mesh['sp'=16,'tp_0'=4,'tp_1'=2] {'tp_0','tp_1'}, dimensions={0} | all-to-all | bytes 8388608 | tf_op jit(solution)/shard_map/all_to_all | solution.py:50
  188.8 0.6 convert_reduce_fusion
  189.4 0.0 copy-done.2
  189.4 0.2 multiply_reduce_fusion
  189.6 0.6 broadcast_in_dim.22
  190.2 3.3 all-to-all-start.1
  193.6 0.0 reduce-scatter.2.cloned.1.call-start
  193.6 0.8 dynamic_slice.3
  194.4 4.5 %all-to-all-done.1 = f32[8,1,512]{2,1,0:T(1,128)S(1)} async-done(((f32[8,1,512]{2,1,0:T(1,128)}), f32[8,1,512]{2,1,0:T(1,128)S(1)}, u32[]{:S(2)}, u32[]{:S(2)}) %all-to-all-start.1) | async-done | bytes 16416 | tf_op jit(solution)/shard_map/all_to_all | solution.py:56
  198.9 0.2 multiply_convert_fusion.1
  199.1 0.2 broadcast_in_dim.23
  199.2 29.1 %all_to_all.22 = bf16[4,512,512]{2,1,0:T(8,128)(2,1)S(1)} all-to-all(bf16[4,512,512]{2,1,0:T(8,128)(2,1)S(1)} %broadcast_in_dim.23), channel_id=1, replica_groups=mesh['sp'=16,'tp_0'=4,'tp_1'=2] {'tp_0'}, dimensions={0} | all-to-all | bytes 4194304 | tf_op jit(solution)/shard_map/all_to_all | solution.py:56
  228.4 0.4 broadcast_in_dim.26
  228.7 7.1 %all_to_all.23 = bf16[2,4,512,512]{3,2,1,0:T(8,128)(2,1)S(1)} all-to-all(bf16[2,4,512,512]{3,2,1,0:T(8,128)(2,1)S(1)} %broadcast_in_dim.26), channel_id=1, replica_groups=mesh['sp'=16,'tp_0'=4,'tp_1'=2] {'tp_1'}, dimensions={0} | all-to-all | bytes 8388608 | tf_op jit(solution)/shard_map/all_to_all | solution.py:56
  235.8 2.4 copy.62
  238.2 6.5 %copy.63 = bf16[512,8,512]{0,2,1:T(8,128)(2,1)} copy(bf16[512,8,512]{2,0,1:T(8,128)(2,1)} %bitcast.95) | data formatting | bytes 8388608 | tf_op jit(solution)/shard_map/transpose | solution.py:64
  244.8 38.8 %all-gather.5.cloned.1.call-done = bf16[4096,4096]{0,1:T(8,128)(2,1)} async-done(((bf16[256,4096]{0,1:T(8,128)(2,1)}), bf16[4096,4096]{0,1:T(8,128)(2,1)}) %all-gather.5.cloned.1.call-update) | async-done | bytes 33554448 | tf_op jit(solution)/shard_map/all_gather | solution.py:23
  283.6 13.7 %multiply_convert_fusion.clone.5 = bf16[512,2048]{1,0:T(8,128)(2,1)S(1)} fusion(bf16[512,4096]{0,1:T(8,128)(2,1)} %bitcast.96, bf16[4096,4096]{0,1:T(8,128)(2,1)} %all-gather.5.cloned.1.call-done), kind=kOutput, calls=%fused_computation.16.clone.clone.clone.2 | convolution fusion | flops 8593080320 | bytes 23068672 | tf_op jit(solution)/shard_map/dot_general | solution.py:170
  297.3 0.0 copy-start.1
  297.3 13.9 %fusion.11 = bf16[512,4096]{1,0:T(8,128)(2,1)} fusion(bf16[4096,4096]{0,1:T(8,128)(2,1)} %all-gather.5.cloned.1.call-done, bf16[512,2048]{1,0:T(8,128)(2,1)S(1)} %multiply_convert_fusion.clone.5), kind=kOutput, calls=%fused_computation.13 | convolution fusion | flops 8592031744 | bytes 23068672 | tf_op jit(solution)/shard_map/dot_general | solution.py:173
  311.2 0.0 reduce-scatter.2.cloned.1.call-update
  311.3 37.3 %reduce-scatter.2.cloned.1.call-done = bf16[512,512]{1,0:T(8,128)(2,1)} async-done(((bf16[512,4096]{1,0:T(8,128)(2,1)}), bf16[512,512]{1,0:T(8,128)(2,1)}) %reduce-scatter.2.cloned.1.call-update) | async-done | bytes 524304 | tf_op jit(solution)/shard_map/reduce_scatter | solution.py:174
  348.6 2.2 add_convert_fusion
  350.8 0.0 copy-done.1
  (8 shorter events, 0.1 us)
Async XLA Ops:
  6.5 126.6 %copy-start = (bf16[256,4096]{1,0:T(8,128)(2,1)S(1)}, bf16[256,4096]{1,0:T(8,128)(2,1)}, u32[]{:S(2)}) copy-start(bf16[256,4096]{1,0:T(8,128)(2,1)} %param.18) | copy-start | bytes 6291460
  6.5 10.1 %copy-start.3 = (bf16[512,256]{1,0:T(8,128)(2,1)S(1)}, bf16[512,256]{1,0:T(8,128)(2,1)}, u32[]{:S(2)}) copy-start(bf16[512,256]{1,0:T(8,128)(2,1)} %param.11) | copy-start | bytes 786436
  6.5 69.9 %all-gather.3.cloned.1.call-start = ((), (), s32[]{:S(2)}) async-start(), calls=%async_computation.5 | async-start | bytes 6684672 | tf_op jit(solution)/shard_map/all_gather | solution.py:34
  10.5 8.4 %copy-start.4 = (f32[128]{0:T(128)S(1)}, f32[128]{0:T(128)}, u32[]{:S(2)}) copy-start(f32[128]{0:T(128)} %param.15) | copy-start | bytes 1540
  12.4 271.2 %all-gather.5.cloned.1.call-start = ((), (), s32[]{:S(2)}) async-start(), calls=%async_computation.6 | async-start | bytes 35651584 | tf_op jit(solution)/shard_map/all_gather | solution.py:23
  134.8 54.5 %copy-start.2 = (bf16[512,512]{1,0:T(8,128)(2,1)S(1)}, bf16[512,512]{1,0:T(8,128)(2,1)}, u32[]{:S(2)}) copy-start(bf16[512,512]{1,0:T(8,128)(2,1)} %param.17) | copy-start | bytes 1572868
  190.2 8.6 %all-to-all-start.1 = ((f32[8,1,512]{2,1,0:T(1,128)}), f32[8,1,512]{2,1,0:T(1,128)S(1)}, u32[]{:S(2)}, u32[]{:S(2)}) async-start(f32[8,1,512]{2,1,0:T(1,128)} %broadcast_in_dim.22), calls=%async_computation.1 | async-start | bytes 32768 | tf_op jit(solution)/shard_map/all_to_all | solution.py:56
  193.6 155.0 %reduce-scatter.2.cloned.1.call-start = ((), (), s32[]{:S(2)}) async-start(), calls=%async_computation.7 | async-start | bytes 4718592 | tf_op jit(solution)/shard_map/reduce_scatter | solution.py:174
  297.3 53.5 %copy-start.1 = (bf16[256,4096]{1,0:T(8,128)(2,1)S(1)}, bf16[256,4096]{1,0:T(8,128)(2,1)}, u32[]{:S(2)}) copy-start(bf16[256,4096]{1,0:T(8,128)(2,1)} %param.18) | copy-start | bytes 6291460
Sparse Core Ops, SparseCore 0:
  12.5 63.8 all-gather.2
  78.5 204.9 all-gather.4
  311.4 37.1 reduce-scatter.1
where the time goes:
time: 358 us; the launch traced here: 357 us
  waiting for transfers between devices  137 us (38%)
  blocking collectives  90.2 us (25%)
  matrix products  63.6 us (18%)
  other arithmetic  30.5 us (9%)
  local copies, waits for them, and re-layouts  18.9 us (5%)
  between operations  13.3 us (4%)
    all_gather x1, waiting for transfers between devices, in_one_piece(): lax.all_gather(both, axis, axis=dim, tiled=True)  56.8 us
    all_to_all x1, blocking collectives, sum_at_owner(): lax.all_to_all(pieces, axis, split_axis=0, concat_axis=0, tiled=True)  53.9 us
    all_gather x1, waiting for transfers between devices, gather_turned(): lax.all_gather(both, axis, axis=0, tiled=True)  38.8 us
    reduce_scatter x1, waiting for transfers between devices, body(): lax.psum_scatter(product.astype(jnp.bfloat16), TP, scatter_dimension=1, t...  37.3 us
    all_to_all x2, blocking collectives, sent_to_all(): return lax.all_to_all(copies, axis, split_axis=0, concat_axis=0, tiled=True)  36.2 us
    dot_general x1, matrix products, body(): jnp.einsum('kgqs,skd->qkgd', probs.astype(jnp.bfloat16), value_piece, pre...  17.6 us
    dot_general x1, matrix products, body(): jnp.einsum('qkgd,skd->kgqs', queries_rot, key_piece, preferred_element_ty...  17.1 us
    reduce_sum x1, other arithmetic, body(): running_sum = jnp.sum(probs, axis=-1)  15.8 us
  transfers between devices with their start and end apart: 4, of which 4 were waited for; matrix products, arithmetic and copies ran while one was open for 22% of the time, Pallas kernels for 0%

commit v1 on v0

v1 whole, which is shorter than its diff:
```python
import functools
import jax
import jax.numpy as jnp
from jax import lax
from jax.experimental import pallas as pl
from jax.experimental.pallas import tpu as pltpu
from jax.sharding import Mesh
from jax.sharding import PartitionSpec as P

D = 4096
FF = 16384
HQ = 16
KV = 8
HD = 128
GRID_W = 64
TOK = 512
HALF = 256
N = 4

norm_eps = 1e-06
rope_base = 10000.0
masked_score = -1e30

MESH = pl.DeviceIdType.MESH
VMEM = pl.BlockSpec(memory_space=pltpu.VMEM)
ANY = pl.BlockSpec(memory_space=pl.ANY)


def shifted(index, by):
    return lax.rem(index + by + N, N)


def send(src, dst, send_sem, recv_sem, device):
    copy = pltpu.make_async_remote_copy(
        src_ref=src,
        dst_ref=dst,
        send_sem=send_sem,
        recv_sem=recv_sem,
        device_id=device,
        device_id_type=MESH,
    )
    copy.start()
    return copy


def arrived(dst, send_sem, recv_sem, device):
    pltpu.make_async_remote_copy(
        src_ref=dst,
        dst_ref=dst,
        send_sem=send_sem,
        recv_sem=recv_sem,
        device_id=device,
        device_id_type=MESH,
    ).wait_recv()


class TorusGather:
    SENDS = 20

    def __init__(self, first, second, piece, start, rows, send_sems, recv_sems, base):
        self.first, self.second = first, second
        self.a, self.b = lax.axis_index(first), lax.axis_index(second)
        self.piece, self.start, self.rows = piece, start, rows
        self.send_sems, self.recv_sems, self.base = send_sems, recv_sems, base
        self.sent = []

    def order(self, j):
        return (self.a, shifted(self.a, -1), shifted(self.a, 1), shifted(self.a, 2))[j]

    def ref(self, a, b, part):
        rows = self.rows // 2
        if part is None:
            return self.piece(a, b, self.start, self.rows)
        return self.piece(a, b, self.start + part * rows, rows)

    def put(self, k, axis, by, a, b, part):
        here = self.ref(a, b, part)
        device = {axis: shifted(lax.axis_index(axis), by)}
        k += self.base
        self.sent.append(send(here, here, self.send_sems.at[k], self.recv_sems.at[k], device))

    def take(self, k, a, b, part):
        k += self.base
        arrived(self.ref(a, b, part), self.send_sems.at[k], self.recv_sems.at[k], {self.first: self.a})

    def spread(self, j):
        self.put(4 + 4 * j, self.second, 1, self.order(j), self.b, None)
        self.put(5 + 4 * j, self.second, -1, self.order(j), self.b, None)

    def begin(self):
        self.put(0, self.first, 1, self.a, self.b, None)
        self.put(1, self.first, -1, self.a, self.b, None)
        self.spread(0)

    def near(self):
        self.take(0, self.order(1), self.b, None)
        self.put(2, self.first, 1, self.order(1), self.b, 0)
        self.spread(1)
        self.take(1, self.order(2), self.b, None)
        self.put(3, self.first, -1, self.order(2), self.b, 1)
        self.spread(2)

    def far(self):
        self.take(2, self.order(3), self.b, 0)
        self.take(3, self.order(3), self.b, 1)
        self.spread(3)

    def pass_on(self, j):
        low, high = shifted(self.b, -1), shifted(self.b, 1)
        self.take(4 + 4 * j, self.order(j), low, None)
        self.put(6 + 4 * j, self.second, 1, self.order(j), low, 0)
        self.take(5 + 4 * j, self.order(j), high, None)
        self.put(7 + 4 * j, self.second, -1, self.order(j), high, 1)

    def last(self, j):
        self.take(6 + 4 * j, self.order(j), shifted(self.b, 2), 0)
        self.take(7 + 4 * j, self.order(j), shifted(self.b, 2), 1)

    def finish(self):
        for copy in self.sent:
            copy.wait_send()


class Exchange:
    SENDS = 6

    def __init__(self, axis, source, target, stage, rows, send_sems, recv_sems, base, beyond=None):
        self.axis, self.me = axis, lax.axis_index(axis)
        self.source, self.target, self.stage, self.rows = source, target, stage, rows
        self.send_sems, self.recv_sems, self.base = send_sems, recv_sems, base
        self.beyond = beyond or {}
        self.sent = []

    def put(self, k, src, dst, by, beyond=True):
        device = {self.axis: shifted(self.me, by)}
        if beyond:
            device.update(self.beyond)
        k += self.base
        self.sent.append(send(src, dst, self.send_sems.at[k], self.recv_sems.at[k], device))

    def take(self, k, dst):
        k += self.base
        arrived(dst, self.send_sems.at[k], self.recv_sems.at[k], {self.axis: self.me})

    def begin(self):
        half = self.rows // 2
        far = shifted(self.me, 2)
        self.put(2, self.source(far, 0, half), self.stage(0), 1, False)
        self.put(3, self.source(far, half, half), self.stage(1), -1, False)
        self.put(0, self.source(shifted(self.me, 1), 0, self.rows), self.target(self.me, 0, self.rows), 1)
        self.put(1, self.source(shifted(self.me, -1), 0, self.rows), self.target(self.me, 0, self.rows), -1)

    def pass_on(self):
        half = self.rows // 2
        self.take(2, self.stage(0))
        self.put(4, self.stage(0), self.target(shifted(self.me, -1), 0, half), 1)
        self.take(3, self.stage(1))
        self.put(5, self.stage(1), self.target(shifted(self.me, 1), half, half), -1)

    def last(self):
        half = self.rows // 2
        self.take(0, self.target(shifted(self.me, -1), 0, self.rows))
        self.take(1, self.target(shifted(self.me, 1), 0, self.rows))
        self.take(4, self.target(shifted(self.me, 2), 0, half))
        self.take(5, self.target(shifted(self.me, 2), half, half))

    def finish(self):
        for copy in self.sent:
            copy.wait_send()


def swapped(u):
    lane = lax.broadcasted_iota(jnp.int32, u.shape, 1)
    ahead = pltpu.roll(u, HD - HD // 4, 1)
    behind = pltpu.roll(u, HD // 4, 1)
    return jnp.where(lax.rem(lane, HD // 2) < HD // 4, ahead, behind)


def rotated(u, gain, cosine, sine):
    u = u.astype(jnp.float32)
    u = u * lax.rsqrt(jnp.mean(u * u, axis=-1, keepdims=True) + norm_eps) * gain
    return (u * cosine + swapped(u) * sine).astype(jnp.bfloat16)


def barrier_with(peers):
    barrier = pltpu.get_barrier_semaphore()
    for peer in peers:
        pl.semaphore_signal(barrier, inc=1, device_id=peer, device_id_type=MESH)
    return lambda: pl.semaphore_wait(barrier, len(peers))


def gather_kernel(
    keys, values, docs, gain, cosine, sine, out_w, up_w, down_w,
    kv, all_docs, out_cols, up_x, down_x,
    up_stage, down_stage, out_stage, send_sems, recv_sems, local_sems,
):
    z, x, y, c = (lax.axis_index(n) for n in ("z", "x", "y", "c"))
    other = 1 - c
    peers = [
        {"z": shifted(z, dz), "x": shifted(x, dx)} for dz in range(N) for dx in range(N) if dz or dx
    ] + [
        {"y": shifted(y, dy), "c": cc} for dy in range(N) for cc in (c, other) if dy or cc is other
    ]
    wait = barrier_with(peers)
    sp = z * N + x
    tp = y * 2 + c
    kv[sp, :, :HD] = rotated(keys[...], gain[...], cosine[...], sine[...])
    kv[sp, :, HD:] = values[...]
    all_docs[sp] = docs[...]
    local = [
        pltpu.make_async_copy(
            out_w.at[:, pl.ds(pl.multiple_of(tp * TOK, TOK), TOK)], out_cols.at[tp], local_sems.at[0]
        ),
        pltpu.make_async_copy(
            up_w.at[:, pl.ds(pl.multiple_of(x * TOK, TOK), TOK)], up_x.at[x], local_sems.at[1]
        ),
        pltpu.make_async_copy(
            down_w.at[pl.ds(pl.multiple_of(x * TOK, TOK), TOK), :], down_x.at[x], local_sems.at[2]
        ),
    ]
    for copy in local:
        copy.start()
    wait()

    def place(zz, xx, start, rows):
        return kv.at[zz * N + xx, pl.ds(start, rows), :]

    gathers = [
        TorusGather("x", "z", lambda a, b, s, r: place(b, a, s, r), 0, TOK, send_sems, recv_sems, 0),
    ]
    ups = Exchange(
        "x",
        lambda to, s, r: up_w.at[pl.ds(s, r), pl.ds(pl.multiple_of(to * TOK, TOK), TOK)],
        lambda who, s, r: up_x.at[who, pl.ds(s, r), :],
        lambda i: up_stage.at[i],
        256, send_sems, recv_sems, 40,
    )
    downs = Exchange(
        "x",
        lambda to, s, r: down_w.at[pl.ds(pl.multiple_of(to * TOK + s, HALF), r), :],
        lambda who, s, r: down_x.at[who, pl.ds(s, r), :],
        lambda i: down_stage.at[i],
        512, send_sems, recv_sems, 46,
    )
    outs = []
    for i, cc in enumerate((c, other)):
        def source(to, s, r, cc=cc):
            return out_w.at[pl.ds(s, r), pl.ds(pl.multiple_of((to * 2 + cc) * TOK, TOK), TOK)]

        def target(who, s, r, cc=cc):
            return out_cols.at[who * 2 + cc, pl.ds(s, r), :]

        outs.append((source, i, cc))
    exchanges = []
    for source, i, cc in outs:
        ex = Exchange(
            "y", source, None, lambda k, i=i: out_stage.at[i, k], 256, send_sems, recv_sems,
            52 + 6 * i, {"c": cc},
        )
        ex.target = lambda who, s, r: out_cols.at[who * 2 + c, pl.ds(s, r), :]
        ex.landed = lambda who, s, r, cc=cc: out_cols.at[who * 2 + cc, pl.ds(s, r), :]
        exchanges.append(ex)

    for g in gathers:
        g.begin()
    for ex in exchanges:
        ex.begin()
    twin = send(
        out_w.at[:, pl.ds(pl.multiple_of((y * 2 + other) * TOK, TOK), TOK)], out_cols.at[tp],
        send_sems.at[64], recv_sems.at[64], {"c": other},
    )
    doc_copies = []
    k = 65
    for dz in range(N):
        for dx in range(N):
            if dz or dx:
                doc_copies.append(
                    send(
                        all_docs.at[sp], all_docs.at[sp], send_sems.at[k], recv_sems.at[k],
                        {"z": shifted(z, dz), "x": shifted(x, dx)},
                    )
                )
                k += 1
    ups.begin()
    downs.begin()
    for g in gathers:
        g.near()
    for g in gathers:
        g.far()
    for ex in exchanges:
        ex.pass_on()
    for j in range(N):
        for g in gathers:
            g.pass_on(j)
        if j == 1:
            ups.pass_on()
            downs.pass_on()
    for j in range(N):
        for g in gathers:
            g.last(j)
    k = 65
    for dz in range(N):
        for dx in range(N):
            if dz or dx:
                arrived(
                    all_docs.at[shifted(z, -dz) * N + shifted(x, -dx)], send_sems.at[k], recv_sems.at[k],
                    {"z": z},
                )
                k += 1
    arrived(out_cols.at[y * 2 + other], send_sems.at[64], recv_sems.at[64], {"c": c})
    for ex in exchanges:
        ex.target, keep = ex.landed, ex.target
        ex.last()
        ex.target = keep
    ups.last()
    downs.last()
    for copy in local:
        copy.wait()
    for done in (*gathers, ups, downs, *exchanges):
        done.finish()
    twin.wait_send()
    for copy in doc_copies:
        copy.wait_send()


def gathered(keys, values, docs, gain, cosine, sine, out_w, up_w, down_w):
    bf = jnp.bfloat16
    return pl.pallas_call(
        gather_kernel,
        out_shape=(
            jax.ShapeDtypeStruct((16, TOK, 2 * HD), bf),
            jax.ShapeDtypeStruct((16, 1, TOK), jnp.int32),
            jax.ShapeDtypeStruct((8, 256, TOK), bf),
            jax.ShapeDtypeStruct((N, 256, TOK), bf),
            jax.ShapeDtypeStruct((N, TOK, 256), bf),
        ),
        in_specs=[VMEM] * 6 + [ANY] * 3,
        out_specs=(VMEM, VMEM, ANY, ANY, ANY),
        scratch_shapes=[
            pltpu.VMEM((2, 128, TOK), bf),
            pltpu.VMEM((2, 256, 256), bf),
            pltpu.VMEM((2, 2, 128, TOK), bf),
            pltpu.SemaphoreType.DMA((80,)),
            pltpu.SemaphoreType.DMA((80,)),
            pltpu.SemaphoreType.DMA((3,)),
        ],
        compiler_params=pltpu.CompilerParams(collective_id=0, has_side_effects=True, vmem_limit_bytes=40 << 20),
        name="gather_kv",
    )(keys, values, docs, gain, cosine, sine, out_w, up_w, down_w)


def attention_kernel(queries, gain, cosine, sine, own_docs, kv, docs, out):
    scale = HD ** (-0.5) * 1.4426950408889634
    everyone = docs[...]
    for t in range(TOK // HALF):
        rows = pl.ds(t * HALF, HALF)
        mine = own_docs[rows, :]
        low = jnp.sum((everyone < jnp.min(mine)).astype(jnp.int32))
        high = jnp.sum((everyone <= jnp.max(mine)).astype(jnp.int32))
        q = [
            rotated(queries[rows, h * HD : (h + 1) * HD], gain[...], cosine[rows, :], sine[rows, :])
            for h in range(2)
        ]

        def step(j, carry):
            k = kv[j, :, :HD]
            v = kv[j, :, HD:]
            same = mine == docs[j]
            after = []
            for h in range(2):
                top, total, weighted = carry[h]
                s = lax.dot_general(q[h], k, (((1,), (1,)), ((), ())), preferred_element_type=jnp.float32)
                s = jnp.where(same, s, masked_score)
                new_top = jnp.maximum(top, jnp.max(s, axis=-1, keepdims=True))
                p = jnp.exp2((s - new_top) * scale)
                fade = jnp.exp2((top - new_top) * scale)
                total = total * fade + jnp.sum(p, axis=-1, keepdims=True)
                weighted = weighted * fade + jnp.dot(
                    p.astype(jnp.bfloat16), v, preferred_element_type=jnp.float32
                )
                after.append((new_top, total, weighted))
            return tuple(after)

        start = (
            jnp.full((HALF, 1), masked_score, jnp.float32),
            jnp.zeros((HALF, 1), jnp.float32),
            jnp.zeros((HALF, HD), jnp.float32),
        )
        ends = lax.fori_loop(lax.div(low, TOK), lax.div(high + (TOK - 1), TOK), step, (start, start))
        for h in range(2):
            top, total, weighted = ends[h]
            out[rows, h * HD : (h + 1) * HD] = (weighted / total).astype(jnp.bfloat16)


def attended_heads(queries, gain, cosine, sine, own_docs, kv, docs):
    return pl.pallas_call(
        attention_kernel,
        out_shape=jax.ShapeDtypeStruct((TOK, 2 * HD), jnp.bfloat16),
        in_specs=[VMEM] * 7,
        out_specs=VMEM,
        compiler_params=pltpu.CompilerParams(vmem_limit_bytes=48 << 20),
        cost_estimate=pl.CostEstimate(flops=4 << 30, bytes_accessed=6 << 20, transcendentals=8 << 20),
        name="attend",
    )(queries, gain, cosine, sine, own_docs, kv, docs)


def tables(sp):
    position = sp * TOK + jnp.arange(TOK, dtype=jnp.int32)
    lane = jnp.arange(HD, dtype=jnp.int32)
    quarter = HD // 4
    inverse_freq = rope_base ** (-(lane % quarter).astype(jnp.float32) / quarter)
    place = jnp.where(
        lane[None, :] < HD // 2, (position // GRID_W)[:, None], (position % GRID_W)[:, None]
    ).astype(jnp.float32)
    angles = place * inverse_freq[None, :]
    sign = jnp.where(lane % (HD // 2) < quarter, -1.0, 1.0)
    return jnp.cos(angles), jnp.sin(angles) * sign[None, :]


class RingGather:
    SENDS = 4

    def __init__(self, axis, piece, own, send_sems, recv_sems, base):
        self.axis, self.me = axis, lax.axis_index(axis)
        self.piece, self.own = piece, own
        self.send_sems, self.recv_sems, self.base = send_sems, recv_sems, base
        self.sent = []

    def put(self, k, src, dst, by):
        device = {self.axis: shifted(self.me, by)}
        k += self.base
        self.sent.append(send(src, dst, self.send_sems.at[k], self.recv_sems.at[k], device))

    def take(self, k, dst):
        k += self.base
        arrived(dst, self.send_sems.at[k], self.recv_sems.at[k], {self.axis: self.me})

    def begin(self):
        self.put(0, self.own, self.piece(self.me, None), 1)
        self.put(1, self.own, self.piece(self.me, None), -1)

    def low(self):
        who = shifted(self.me, -1)
        self.take(0, self.piece(who, None))
        self.put(2, self.piece(who, 0), self.piece(who, 0), 1)

    def high(self):
        who = shifted(self.me, 1)
        self.take(1, self.piece(who, None))
        self.put(3, self.piece(who, 1), self.piece(who, 1), -1)

    def far(self):
        who = shifted(self.me, 2)
        self.take(2, self.piece(who, 0))
        self.take(3, self.piece(who, 1))

    def finish(self):
        for copy in self.sent:
            copy.wait_send()


class TorusReduce:
    SENDS = 20

    def __init__(self, first, second, piece, start, rows, bufs, send_sems, recv_sems, base):
        self.first, self.second = first, second
        self.a, self.b = lax.axis_index(first), lax.axis_index(second)
        self.piece, self.start, self.rows = piece, start, rows
        self.far_first, self.near_first, self.far_second, self.near_second = bufs
        self.send_sems, self.recv_sems, self.base = send_sems, recv_sems, base
        self.sent = []

    def dest(self, j):
        return shifted(self.b, (2, 1, -1, 0)[j])

    def ref(self, a, b, part):
        rows = self.rows // 2
        if part is None:
            return self.piece(a, b, self.start, self.rows)
        return self.piece(a, b, self.start + part * rows, rows)

    def put(self, k, axis, by, src, dst):
        device = {axis: shifted(lax.axis_index(axis), by)}
        k += self.base
        self.sent.append(send(src, dst, self.send_sems.at[k], self.recv_sems.at[k], device))

    def take(self, k, dst):
        k += self.base
        arrived(dst, self.send_sems.at[k], self.recv_sems.at[k], {self.first: self.a})

    @staticmethod
    def add(into, *others):
        total = into[...].astype(jnp.float32)
        for other in others:
            total = total + other[...].astype(jnp.float32)
        into[...] = total.astype(into.dtype)

    def far(self, j):
        a, b = shifted(self.a, 2), self.dest(j)
        self.put(4 * j, self.first, 1, self.ref(a, b, 0), self.far_first.at[0, j])
        self.put(4 * j + 1, self.first, -1, self.ref(a, b, 1), self.far_first.at[1, j])

    def up(self, j):
        a, b = shifted(self.a, 1), self.dest(j)
        self.take(4 * j, self.far_first.at[0, j])
        self.add(self.ref(a, b, 0), self.far_first.at[0, j])
        self.put(4 * j + 2, self.first, 1, self.ref(a, b, None), self.near_first.at[0, j])

    def down(self, j):
        a, b = shifted(self.a, -1), self.dest(j)
        self.take(4 * j + 1, self.far_first.at[1, j])
        self.add(self.ref(a, b, 1), self.far_first.at[1, j])
        self.put(4 * j + 3, self.first, -1, self.ref(a, b, None), self.near_first.at[1, j])

    def own(self, j):
        self.take(4 * j + 2, self.near_first.at[0, j])
        self.take(4 * j + 3, self.near_first.at[1, j])
        self.add(self.ref(self.a, self.dest(j), None), self.near_first.at[0, j], self.near_first.at[1, j])

    def second_far(self):
        b = shifted(self.b, 2)
        self.put(16, self.second, 1, self.ref(self.a, b, 0), self.far_second.at[0])
        self.put(17, self.second, -1, self.ref(self.a, b, 1), self.far_second.at[1])

    def second_up(self):
        b = shifted(self.b, 1)
        self.take(16, self.far_second.at[0])
        self.add(self.ref(self.a, b, 0), self.far_second.at[0])
        self.put(18, self.second, 1, self.ref(self.a, b, None), self.near_second.at[0])

    def second_down(self):
        b = shifted(self.b, -1)
        self.take(17, self.far_second.at[1])
        self.add(self.ref(self.a, b, 1), self.far_second.at[1])
        self.put(19, self.second, -1, self.ref(self.a, b, None), self.near_second.at[1])

    def total(self):
        self.take(18, self.near_second.at[0])
        self.take(19, self.near_second.at[1])
        total = self.ref(self.a, self.b, None)[...].astype(jnp.float32)
        total = total + self.near_second[0].astype(jnp.float32)
        return total + self.near_second[1].astype(jnp.float32)

    def finish(self):
        for copy in self.sent:
            copy.wait_send()


def layer_kernel(
    att, out_cols, residual, gains, up_x, down_x, mixed,
    x_all, up_all, down_all, sums, theirs, stream, hidden, squared, squares,
    far_first, near_first, far_second, near_second, send_sems, recv_sems, local_sems,
):
    z, x, y, c = (lax.axis_index(n) for n in ("z", "x", "y", "c"))
    other = 1 - c
    tp = y * 2 + c
    group = [{"y": shifted(y, dy), "c": cc} for dy in range(N) for cc in (c, other) if dy or cc is other]
    wait = barrier_with(
        group + [{"z": shifted(z, 1)}, {"z": shifted(z, -1)}, {"x": shifted(x, 1)}, {"x": shifted(x, -1)}]
    )

    def att_slot(t, part):
        rows = pl.ds(0, TOK) if part is None else pl.ds(part * HALF, HALF)
        return sums.at[0, lax.div(t, 4), lax.rem(t, 4), rows, pl.ds(0, 256)]

    def col_slot(t):
        return theirs.at[lax.div(t, 4), lax.rem(t, 4), pl.ds(0, 256), :]

    local = [
        pltpu.make_async_copy(out_cols.at[t], col_slot(t), local_sems.at[t]) for t in range(8)
    ]
    for copy in local:
        copy.start()
    weights = [
        pltpu.make_async_copy(up_x, up_all.at[z], local_sems.at[8]),
        pltpu.make_async_copy(down_x, down_all.at[z], local_sems.at[9]),
    ]
    for copy in weights:
        copy.start()
    wait()

    heads = RingGather("y", lambda who, part: att_slot(who * 2 + c, part), att, send_sems, recv_sems, 0)
    heads.begin()
    handed = []

    def hand(k, src, dst):
        handed.append(send(src, dst, send_sems.at[k], recv_sems.at[k], {"c": other}))

    def taken(k, dst):
        arrived(dst, send_sems.at[k], recv_sems.at[k], {"c": c})

    hand(4, att, att_slot(tp, None))

    def half_of(ref, z_at, part):
        at = ref.at[z_at]
        return at if part is None else at.at[pl.ds(2 * part, 2)]

    ups = RingGather("z", lambda who, part: half_of(up_all, who, part), up_x, send_sems, recv_sems, 8)
    downs = RingGather("z", lambda who, part: half_of(down_all, who, part), down_x, send_sems, recv_sems, 12)
    ups.begin()
    downs.begin()
    for copy in local:
        copy.wait()

    def project(t, piece):
        part = jnp.dot(piece[...], col_slot(t)[...], preferred_element_type=jnp.float32)
        stream[...] += part.astype(jnp.bfloat16).astype(jnp.float32)

    def project_slot(t):
        project(t, att_slot(t, None))

    y_low, y_high, y_far = shifted(y, -1), shifted(y, 1), shifted(y, 2)
    stream[...] = residual[...].astype(jnp.float32)
    project(tp, att)
    heads.low()
    hand(5, att_slot(y_low * 2 + c, None), att_slot(y_low * 2 + c, None))
    heads.high()
    hand(6, att_slot(y_high * 2 + c, None), att_slot(y_high * 2 + c, None))
    taken(4, att_slot(y * 2 + other, None))
    project_slot(y * 2 + other)
    project_slot(y_low * 2 + c)
    project_slot(y_high * 2 + c)
    heads.far()
    hand(7, att_slot(y_far * 2 + c, None), att_slot(y_far * 2 + c, None))
    taken(5, att_slot(y_low * 2 + other, None))
    project_slot(y_low * 2 + other)
    taken(6, att_slot(y_high * 2 + other, None))
    project_slot(y_high * 2 + other)
    project_slot(y_far * 2 + c)
    taken(7, att_slot(y_far * 2 + other, None))
    project_slot(y_far * 2 + other)

    heads.finish()
    for copy in handed:
        copy.wait_send()
    handed.clear()

    whole = stream[...]
    partial = jnp.sum(whole * whole, axis=-1, keepdims=True)
    squares[tp] = jnp.transpose(jnp.broadcast_to(partial, (TOK, HD)))[:8]
    square_copies = [
        send(squares.at[tp], squares.at[tp], send_sems.at[16 + i], recv_sems.at[16 + i], peer)
        for i, peer in enumerate(group)
    ]
    i = 0
    for dy in range(N):
        for cc in (c, other):
            if dy or cc is other:
                arrived(squares.at[shifted(y, -dy) * 2 + cc], send_sems.at[16 + i], recv_sems.at[16 + i], {"c": c})
                i += 1
    full = squares[0]
    for t in range(1, 8):
        full = full + squares[t]
    full = jnp.transpose(jnp.broadcast_to(full[:1], (HD, TOK)))
    inverse = lax.rsqrt(full[:, :1] / D + norm_eps)
    x_all[x, tp] = (stream[...] * inverse * gains[tp]).astype(jnp.bfloat16)

    def place(xx, yy, start, rows):
        return x_all.at[xx, yy * 2 + c, pl.ds(start, rows), :]

    gathers = [
        TorusGather("y", "x", lambda a, b, s, r: place(b, a, s, r), 0, HALF, send_sems, recv_sems, 24),
        TorusGather("x", "y", place, HALF, HALF, send_sems, recv_sems, 44),
    ]

    def share(g, n, j, a, b):
        ref = g.ref(a, b, None)
        hand(64 + 16 * n + j, ref, ref)

    for g in gathers:
        g.begin()
    for n, g in enumerate(gathers):
        share(g, n, 0, g.a, g.b)
    for n, g in enumerate(gathers):
        g.near()
        share(g, n, 4, g.order(1), g.b)
        share(g, n, 8, g.order(2), g.b)
    for n, g in enumerate(gathers):
        g.far()
        share(g, n, 12, g.order(3), g.b)
    for j in range(N):
        for n, g in enumerate(gathers):
            g.pass_on(j)
            share(g, n, 4 * j + 1, g.order(j), shifted(g.b, -1))
            share(g, n, 4 * j + 2, g.order(j), shifted(g.b, 1))
        if j == 1:
            ups.low()
            ups.high()
    for j in range(N):
        for n, g in enumerate(gathers):
            g.last(j)
            share(g, n, 4 * j + 3, g.order(j), shifted(g.b, 2))
    downs.low()
    downs.high()
    for n, g in enumerate(gathers):
        for j in range(N):
            for i, by in enumerate((0, -1, 1, 2)):
                a, b = g.order(j), shifted(g.b, by)
                xx, yy = (b, a) if n == 0 else (a, b)
                taken(
                    64 + 16 * n + 4 * j + i,
                    x_all.at[xx, yy * 2 + other, pl.ds(n * HALF, HALF), :],
                )
    for copy in weights:
        copy.wait()
    ups.far()
    downs.far()

    def feed(i, xx):
        hidden[...] = jnp.zeros_like(hidden)

        @pl.loop(0, 8)
        def _(t):
            w = up_all[lax.div(t, 2), pl.ds(2 * lax.rem(t, 2), 2)].reshape(TOK, TOK)
            hidden[...] += jnp.dot(x_all[xx, t], w, preferred_element_type=jnp.float32)

        positive = jnp.maximum(hidden[...], 0.0)
        squared[...] = (positive * positive).astype(jnp.bfloat16)

        @pl.loop(0, 8)
        def _(t):
            for part in range(2):
                w = down_all[lax.div(t, 2), 2 * lax.rem(t, 2) + part]
                sums[lax.rem(t, 2), xx, lax.div(t, 2), :, part * 256 : (part + 1) * 256] = jnp.dot(
                    squared[...], w, preferred_element_type=jnp.float32
                ).astype(jnp.bfloat16)

        hand(96 + i, sums.at[other, xx], theirs.at[xx])

    def joined(i, xx):
        taken(96 + i, theirs.at[xx])

        @pl.loop(0, N)
        def _(yy):
            TorusReduce.add(sums.at[c, xx, yy], theirs.at[xx, yy])

    def sum_place(xx, yy, start, rows):
        return sums.at[c, xx, yy, pl.ds(start, rows), :]

    def bufs(n):
        return far_first.at[n], near_first.at[n], far_second.at[n], near_second.at[n]

    rows_x = TorusReduce("x", "y", sum_place, 0, HALF, bufs(0), send_sems, recv_sems, 100)
    rows_y = TorusReduce(
        "y", "x", lambda a, b, s, r: sum_place(b, a, s, r), HALF, HALF, bufs(1), send_sems, recv_sems, 120
    )
    blocks = [rows_y.dest(j) for j in range(N)]
    feed(0, blocks[0])
    feed(1, blocks[1])
    joined(0, blocks[0])
    for j in range(N):
        rows_x.far(j)
    rows_y.far(0)
    feed(2, blocks[2])
    joined(1, blocks[1])
    rows_y.far(1)
    for j in range(N):
        rows_x.up(j)
    rows_y.up(0)
    rows_y.down(0)
    feed(3, blocks[3])
    joined(2, blocks[2])
    rows_y.far(2)
    for j in range(N):
        rows_x.down(j)
    rows_y.up(1)
    rows_y.down(1)
    joined(3, blocks[3])
    rows_y.far(3)
    rows_y.up(2)
    rows_y.down(2)
    rows_y.up(3)
    rows_y.down(3)
    for j in range(N):
        for r in (rows_x, rows_y):
            r.own(j)
            if j == 0:
                r.second_far()
            if j == 1:
                r.second_up()
            if j == 2:
                r.second_down()
    mixed[:HALF, :] = (stream[:HALF, :] + rows_x.total()).astype(jnp.bfloat16)
    mixed[HALF:, :] = (stream[HALF:, :] + rows_y.total()).astype(jnp.bfloat16)
    for done in (ups, downs, *gathers, rows_x, rows_y):
        done.finish()
    for copy in (*handed, *square_copies):
        copy.wait_send()


def layer(att, out_cols, residual, gains, up_x, down_x):
    bf = jnp.bfloat16
    return pl.pallas_call(
        layer_kernel,
        out_shape=jax.ShapeDtypeStruct((TOK, TOK), bf),
        in_specs=[VMEM, ANY, VMEM, VMEM, ANY, ANY],
        out_specs=VMEM,
        scratch_shapes=[
            pltpu.VMEM((N, 8, TOK, TOK), bf),
            pltpu.VMEM((N, N, 256, TOK), bf),
            pltpu.VMEM((N, N, TOK, 256), bf),
            pltpu.VMEM((2, N, N, TOK, TOK), bf),
            pltpu.VMEM((N, N, TOK, TOK), bf),
            pltpu.VMEM((TOK, TOK), jnp.float32),
            pltpu.VMEM((TOK, TOK), jnp.float32),
            pltpu.VMEM((TOK, TOK), bf),
            pltpu.VMEM((8, 8, TOK), jnp.float32),
            pltpu.VMEM((2, 2, N, 128, TOK), bf),
            pltpu.VMEM((2, 2, N, HALF, TOK), bf),
            pltpu.VMEM((2, 2, 128, TOK), bf),
            pltpu.VMEM((2, 2, HALF, TOK), bf),
            pltpu.SemaphoreType.DMA((140,)),
            pltpu.SemaphoreType.DMA((140,)),
            pltpu.SemaphoreType.DMA((10,)),
        ],
        compiler_params=pltpu.CompilerParams(
            collective_id=1, has_side_effects=True, vmem_limit_bytes=67043328
        ),
        name="layer",
    )(att, out_cols, residual, gains, up_x, down_x)


def body(
    queries, keys, values, documents, query_gain, key_gain, residual, out_weight, norm_gain, up_weight, down_weight
):
    cosine, sine = tables(lax.axis_index(("z", "x")))
    kv, docs, out_cols, up_x, down_x = gathered(
        keys, values, documents.reshape(1, TOK), key_gain.reshape(1, HD), cosine, sine,
        out_weight, up_weight, down_weight,
    )
    att = attended_heads(
        queries, query_gain.reshape(1, HD), cosine, sine, documents.reshape(TOK, 1), kv, docs
    )
    return layer(att, out_cols, residual, norm_gain.reshape(8, 1, TOK), up_x, down_x)


def solution(mesh):
    split = Mesh(mesh.devices.reshape(N, N, N, 2), ("z", "x", "y", "c"))
    sp, tp = ("z", "x"), ("y", "c")
    return jax.shard_map(
        body,
        mesh=split,
        in_specs=(
            P(sp, tp), P(sp, tp), P(sp, tp), P(sp), P(), P(), P(sp, tp), P(tp, None), P(), P(sp, tp), P(tp, sp),
        ),
        out_specs=P(sp, tp),
        check_vma=False,
    )
```

time: 358 us -> 240 us (0.67)
  Pallas kernels: 0 us -> 223 us
  waiting for transfers between devices: 137 us -> 0 us
  blocking collectives: 90.2 us -> 0 us
  matrix products: 63.6 us -> 0 us
  other arithmetic: 30.5 us -> 1.05 us
  between operations: 13.3 us -> 0.08 us
  local copies, waits for them, and re-layouts: 18.9 us -> 13.9 us
    pallas_call x0 -> x3, Pallas kernels: none -> 223 us  [the longest x1 151 us: layer(): pl.pallas_call(layer_kernel, out_shape=jax.ShapeDtypeStruct((TOK, TOK), b...]
    all_gather x2 -> x0, waiting for transfers between devices: 95.6 us -> none  [the longest x1 56.8 us: in_one_piece(): lax.all_gather(both, axis, axis=dim, tiled=True)]
    all_to_all x3 -> x0, blocking collectives: 90.2 us -> none  [the longest x1 53.9 us: sum_at_owner(): lax.all_to_all(pieces, axis, split_axis=0, concat_axis=0, tiled=True)]
    dot_general x5 -> x0, matrix products: 63.6 us -> none  [the longest x1 17.6 us: body(): jnp.einsum('kgqs,skd->qkgd', probs.astype(jnp.bfloat16), value_piece, pre...]
    reduce_scatter x1 -> x0, waiting for transfers between devices: 37.3 us -> none  [body(): lax.psum_scatter(product.astype(jnp.bfloat16), TP, scatter_dimension=1, t...]
    reduce_sum x6 -> x0, other arithmetic: 16.8 us -> none  [the longest x1 15.8 us: body(): running_sum = jnp.sum(probs, axis=-1)]
    unnamed x13 -> x27, local copies, waits for them, and re-layouts: 2.83 us -> 13.1 us
    transpose x1 -> x0, local copies, waits for them, and re-layouts: 6.54 us -> none  [joined_along(): pieces = jnp.moveaxis(pieces, 0, dim)]
  transfers between devices with their start and end apart: 4 -> 0, of which waited for: 4 -> 0; matrix products, arithmetic and copies ran while one was open for 22% -> 0% of each run, Pallas kernels for 0% -> 0%
where the time goes in v1:
time: 240 us; the launch traced here: 238 us
  Pallas kernels  223 us (93%)
  local copies, waits for them, and re-layouts  13.9 us (6%)
    pallas_call x1, Pallas kernels, layer(): pl.pallas_call(layer_kernel, out_shape=jax.ShapeDtypeStruct((TOK, TOK), b...  151 us
    pallas_call x1, Pallas kernels, gathered(): pl.pallas_call(gather_kernel, out_shape=(jax.ShapeDtypeStruct((16, TOK, 2...  55.7 us
    pallas_call x1, Pallas kernels, attended_heads(): pl.pallas_call(attention_kernel, out_shape=jax.ShapeDtypeStruct((TOK, 2 *...  16.2 us
    unnamed x27, local copies, waits for them, and re-layouts  13.1 us

profile of v1, /device:TPU:0, one launch (start us, length us, event | category | flops | bytes accessed | tf_op | source)
XLA Modules:
  0.0 238.0 jit_solution(8917148758215344408)
XLA Ops:
  0.0 0.8 copy.12.own_docs
  0.9 1.0 sine_multiply_fusion
  1.9 0.0 copy-start
  1.9 1.6 copy-done
  3.5 0.0 copy-start.2
  3.5 1.2 copy-done.2
  4.7 0.0 copy-start.3
  4.7 1.2 copy-done.3
  5.9 0.0 copy-start.7
  5.9 0.9 copy-done.7
  6.8 0.0 copy-start.8
  6.8 0.9 copy-done.8
  7.7 0.0 copy-start.9
  7.7 0.7 copy-done.9
  8.4 0.0 copy-start.10
  8.4 0.7 copy-done.10
  9.1 0.0 copy-start.11
  9.1 0.0 copy-start.12
  9.1 55.7 %gather_kv.1 = (bf16[16,512,256]{2,1,0:T(8,128)(2,1)S(1)}, s32[16,1,512]{2,1,0:T(1,128)S(1)}, bf16[8,256,512]{2,1,0:T(8,128)(2,1)S(1)}, bf16[4,256,512]{2,1,0:T(8,128)(2,1)S(1)}, bf16[4,512,256]{2,1,0:T(8,128)(2,1)S(1)}) custom-call(bf16[512,128]{1,0:T(8,128)(2,1)S(1)} %copy-done.7, bf16[512,128]{1,0:T(8,128)(2,1)S(1)} %copy-done.8, s32[1,512]{1,0:T(1,128)S(1)} %bitcast.6, ...), custom_call_target="tpu_custom_call" | custom-call | tf_op jit(solution)/shard_map/gather_kv/pallas_call | solution.py:328
  64.8 0.0 copy-start.1
  64.8 1.3 copy-done.1
  66.1 0.0 copy-start.4
  66.1 1.0 copy-done.4
  67.1 0.0 copy-start.5
  67.1 1.0 copy-done.5
  68.1 0.0 copy-done.11
  68.1 0.0 copy-done.12
  68.1 16.2 %attend.1.att = bf16[512,256]{1,0:T(8,128)(2,1)S(1)} custom-call(bf16[512,256]{1,0:T(8,128)(2,1)S(1)} %copy-done.11, f32[1,128]{1,0:T(1,128)S(1)} %bitcast.8, f32[512,128]{1,0:T(8,128)S(1)} %get-tuple-element.16.cosine, f32[512,128]{1,0:T(8,128)S(1)} %get-tuple-element.15.sine, s32[512,1]{1,0:T(8,128)S(1)} %copy.12.own_docs, ...), custom_call_target="tpu_custom_call" | custom-call | flops 4294967296 | bytes 6291456 | tf_op jit(solution)/shard_map/attend/pallas_call | solution.py:396
  84.3 0.0 copy-start.6
  84.3 0.7 copy-done.6
  85.0 151.2 %layer.1 = bf16[512,512]{1,0:T(8,128)(2,1)} custom-call(bf16[512,256]{1,0:T(8,128)(2,1)} %copy-done.6, bf16[8,256,512]{2,1,0:T(8,128)(2,1)} %copy-done.1, bf16[512,512]{1,0:T(8,128)(2,1)} %residual.1, f32[8,1,512]{2,1,0:T(1,128)} %bitcast.9, bf16[4,256,512]{2,1,0:T(8,128)(2,1)} %copy-done.4, bf16[4,512,256]{2,1,0:T(8,128)(2,1)} %copy-done.5), custom_call_target="tpu_custom_call" | custom-call | tf_op jit(solution)/shard_map/layer/pallas_call | solution.py:793
  236.2 1.9 copy.14
  (3 shorter events, 0.0 us)
Async XLA Ops:
  1.9 1.6 copy-start
  3.5 1.2 copy-start.2
  4.7 1.2 copy-start.3
  5.9 0.9 copy-start.7
  6.8 0.9 copy-start.8
  7.7 0.7 copy-start.9
  8.4 0.7 copy-start.10
  9.1 59.0 %copy-start.11 = (bf16[512,256]{1,0:T(8,128)(2,1)S(1)}, bf16[512,256]{1,0:T(8,128)(2,1)}, u32[]{:S(2)}) copy-start(bf16[512,256]{1,0:T(8,128)(2,1)} %queries.1) | copy-start | bytes 786436
  9.1 59.0 %copy-start.12 = (f32[128]{0:T(128)S(1)}, f32[128]{0:T(128)}, u32[]{:S(2)}) copy-start(f32[128]{0:T(128)} %param.15) | copy-start | bytes 1540
  64.8 1.3 copy-start.1
  66.1 1.0 copy-start.4
  67.1 1.0 copy-start.5
  84.3 0.7 copy-start.6

commit v2 on v1

v2 whole, which is shorter than its diff:
```python
import functools
import jax
import jax.numpy as jnp
from jax import lax
from jax.experimental import pallas as pl
from jax.experimental.pallas import tpu as pltpu
from jax.sharding import Mesh
from jax.sharding import PartitionSpec as P

D = 4096
FF = 16384
HQ = 16
KV = 8
HD = 128
GRID_W = 64
TOK = 512
HALF = 256
N = 4

norm_eps = 1e-06
rope_base = 10000.0
masked_score = -1e30
query_mark = 128.0
key_mark = 96.0

MESH = pl.DeviceIdType.MESH
VMEM = pl.BlockSpec(memory_space=pltpu.VMEM)
ANY = pl.BlockSpec(memory_space=pl.ANY)


def shifted(index, by):
    return lax.rem(index + by + N, N)


def send(src, dst, send_sem, recv_sem, device):
    copy = pltpu.make_async_remote_copy(
        src_ref=src,
        dst_ref=dst,
        send_sem=send_sem,
        recv_sem=recv_sem,
        device_id=device,
        device_id_type=MESH,
    )
    copy.start()
    return copy


def arrived(dst, send_sem, recv_sem, device):
    pltpu.make_async_remote_copy(
        src_ref=dst,
        dst_ref=dst,
        send_sem=send_sem,
        recv_sem=recv_sem,
        device_id=device,
        device_id_type=MESH,
    ).wait_recv()


class TorusGather:
    SENDS = 20

    def __init__(self, first, second, piece, start, rows, send_sems, recv_sems, base):
        self.first, self.second = first, second
        self.a, self.b = lax.axis_index(first), lax.axis_index(second)
        self.piece, self.start, self.rows = piece, start, rows
        self.send_sems, self.recv_sems, self.base = send_sems, recv_sems, base
        self.sent = []

    def order(self, j):
        return (self.a, shifted(self.a, -1), shifted(self.a, 1), shifted(self.a, 2))[j]

    def ref(self, a, b, part):
        rows = self.rows // 2
        if part is None:
            return self.piece(a, b, self.start, self.rows)
        return self.piece(a, b, self.start + part * rows, rows)

    def put(self, k, axis, by, a, b, part):
        here = self.ref(a, b, part)
        device = {axis: shifted(lax.axis_index(axis), by)}
        k += self.base
        self.sent.append(send(here, here, self.send_sems.at[k], self.recv_sems.at[k], device))

    def take(self, k, a, b, part):
        k += self.base
        arrived(self.ref(a, b, part), self.send_sems.at[k], self.recv_sems.at[k], {self.first: self.a})

    def spread(self, j):
        self.put(4 + 4 * j, self.second, 1, self.order(j), self.b, None)
        self.put(5 + 4 * j, self.second, -1, self.order(j), self.b, None)

    def begin(self):
        self.put(0, self.first, 1, self.a, self.b, None)
        self.put(1, self.first, -1, self.a, self.b, None)
        self.spread(0)

    def near(self):
        self.take(0, self.order(1), self.b, None)
        self.put(2, self.first, 1, self.order(1), self.b, 0)
        self.spread(1)
        self.take(1, self.order(2), self.b, None)
        self.put(3, self.first, -1, self.order(2), self.b, 1)
        self.spread(2)

    def far(self):
        self.take(2, self.order(3), self.b, 0)
        self.take(3, self.order(3), self.b, 1)
        self.spread(3)

    def pass_on(self, j):
        low, high = shifted(self.b, -1), shifted(self.b, 1)
        self.take(4 + 4 * j, self.order(j), low, None)
        self.put(6 + 4 * j, self.second, 1, self.order(j), low, 0)
        self.take(5 + 4 * j, self.order(j), high, None)
        self.put(7 + 4 * j, self.second, -1, self.order(j), high, 1)

    def last(self, j):
        self.take(6 + 4 * j, self.order(j), shifted(self.b, 2), 0)
        self.take(7 + 4 * j, self.order(j), shifted(self.b, 2), 1)

    def finish(self):
        for copy in self.sent:
            copy.wait_send()


class Exchange:
    SENDS = 6

    def __init__(self, axis, source, target, stage, rows, send_sems, recv_sems, base, beyond=None):
        self.axis, self.me = axis, lax.axis_index(axis)
        self.source, self.target, self.stage, self.rows = source, target, stage, rows
        self.send_sems, self.recv_sems, self.base = send_sems, recv_sems, base
        self.beyond = beyond or {}
        self.sent = []

    def put(self, k, src, dst, by, beyond=True):
        device = {self.axis: shifted(self.me, by)}
        if beyond:
            device.update(self.beyond)
        k += self.base
        self.sent.append(send(src, dst, self.send_sems.at[k], self.recv_sems.at[k], device))

    def take(self, k, dst):
        k += self.base
        arrived(dst, self.send_sems.at[k], self.recv_sems.at[k], {self.axis: self.me})

    def begin(self):
        half = self.rows // 2
        far = shifted(self.me, 2)
        self.put(2, self.source(far, 0, half), self.stage(0), 1, False)
        self.put(3, self.source(far, half, half), self.stage(1), -1, False)
        self.put(0, self.source(shifted(self.me, 1), 0, self.rows), self.target(self.me, 0, self.rows), 1)
        self.put(1, self.source(shifted(self.me, -1), 0, self.rows), self.target(self.me, 0, self.rows), -1)

    def pass_on(self):
        half = self.rows // 2
        self.take(2, self.stage(0))
        self.put(4, self.stage(0), self.target(shifted(self.me, -1), 0, half), 1)
        self.take(3, self.stage(1))
        self.put(5, self.stage(1), self.target(shifted(self.me, 1), half, half), -1)

    def last(self):
        half = self.rows // 2
        self.take(0, self.target(shifted(self.me, -1), 0, self.rows))
        self.take(1, self.target(shifted(self.me, 1), 0, self.rows))
        self.take(4, self.target(shifted(self.me, 2), 0, half))
        self.take(5, self.target(shifted(self.me, 2), half, half))

    def finish(self):
        for copy in self.sent:
            copy.wait_send()


def swapped(u):
    lane = lax.broadcasted_iota(jnp.int32, u.shape, 1)
    ahead = pltpu.roll(u, HD - HD // 4, 1)
    behind = pltpu.roll(u, HD // 4, 1)
    return jnp.where(lax.rem(lane, HD // 2) < HD // 4, ahead, behind)


def rotated(u, gain, cosine, sine):
    u = u.astype(jnp.float32)
    u = u * lax.rsqrt(jnp.mean(u * u, axis=-1, keepdims=True) + norm_eps) * gain
    return (u * cosine + swapped(u) * sine).astype(jnp.bfloat16)


def barrier_with(peers):
    barrier = pltpu.get_barrier_semaphore()
    for peer in peers:
        pl.semaphore_signal(barrier, inc=1, device_id=peer, device_id_type=MESH)
    return lambda: pl.semaphore_wait(barrier, len(peers))


def tables(sp):
    position = sp * TOK + jnp.arange(TOK, dtype=jnp.int32)
    lane = jnp.arange(HD, dtype=jnp.int32)
    quarter = HD // 4
    inverse_freq = rope_base ** (-(lane % quarter).astype(jnp.float32) / quarter)
    place = jnp.where(
        lane[None, :] < HD // 2, (position // GRID_W)[:, None], (position % GRID_W)[:, None]
    ).astype(jnp.float32)
    angles = place * inverse_freq[None, :]
    sign = jnp.where(lane % (HD // 2) < quarter, -1.0, 1.0)
    return jnp.cos(angles), jnp.sin(angles) * sign[None, :]


class RingGather:
    SENDS = 4

    def __init__(self, axis, piece, own, send_sems, recv_sems, base):
        self.axis, self.me = axis, lax.axis_index(axis)
        self.piece, self.own = piece, own
        self.send_sems, self.recv_sems, self.base = send_sems, recv_sems, base
        self.sent = []

    def put(self, k, src, dst, by):
        device = {self.axis: shifted(self.me, by)}
        k += self.base
        self.sent.append(send(src, dst, self.send_sems.at[k], self.recv_sems.at[k], device))

    def take(self, k, dst):
        k += self.base
        arrived(dst, self.send_sems.at[k], self.recv_sems.at[k], {self.axis: self.me})

    def begin(self):
        self.put(0, self.own, self.piece(self.me, None), 1)
        self.put(1, self.own, self.piece(self.me, None), -1)

    def low(self):
        who = shifted(self.me, -1)
        self.take(0, self.piece(who, None))
        self.put(2, self.piece(who, 0), self.piece(who, 0), 1)

    def high(self):
        who = shifted(self.me, 1)
        self.take(1, self.piece(who, None))
        self.put(3, self.piece(who, 1), self.piece(who, 1), -1)

    def far(self):
        who = shifted(self.me, 2)
        self.take(2, self.piece(who, 0))
        self.take(3, self.piece(who, 1))

    def finish(self):
        for copy in self.sent:
            copy.wait_send()


class TorusReduce:
    SENDS = 20

    def __init__(self, first, second, piece, start, rows, bufs, send_sems, recv_sems, base):
        self.first, self.second = first, second
        self.a, self.b = lax.axis_index(first), lax.axis_index(second)
        self.piece, self.start, self.rows = piece, start, rows
        self.buf = bufs
        self.send_sems, self.recv_sems, self.base = send_sems, recv_sems, base
        self.sent = []

    def dest(self, j):
        return shifted(self.b, (2, 1, -1, 0)[j])

    def ref(self, a, b, part):
        rows = self.rows // 2
        if part is None:
            return self.piece(a, b, self.start, self.rows)
        return self.piece(a, b, self.start + part * rows, rows)

    def put(self, k, axis, by, src, dst):
        device = {axis: shifted(lax.axis_index(axis), by)}
        k += self.base
        self.sent.append(send(src, dst, self.send_sems.at[k], self.recv_sems.at[k], device))

    def take(self, k, dst):
        k += self.base
        arrived(dst, self.send_sems.at[k], self.recv_sems.at[k], {self.first: self.a})

    @staticmethod
    def add(into, *others):
        total = into[...].astype(jnp.float32)
        for other in others:
            total = total + other[...].astype(jnp.float32)
        into[...] = total.astype(into.dtype)

    def far(self, j):
        a, b = shifted(self.a, 2), self.dest(j)
        self.put(4 * j, self.first, 1, self.ref(a, b, 0), self.buf("far_first", 0, j))
        self.put(4 * j + 1, self.first, -1, self.ref(a, b, 1), self.buf("far_first", 1, j))

    def up(self, j):
        a, b = shifted(self.a, 1), self.dest(j)
        self.take(4 * j, self.buf("far_first", 0, j))
        self.add(self.ref(a, b, 0), self.buf("far_first", 0, j))
        self.put(4 * j + 2, self.first, 1, self.ref(a, b, None), self.buf("near_first", 0, j))

    def down(self, j):
        a, b = shifted(self.a, -1), self.dest(j)
        self.take(4 * j + 1, self.buf("far_first", 1, j))
        self.add(self.ref(a, b, 1), self.buf("far_first", 1, j))
        self.put(4 * j + 3, self.first, -1, self.ref(a, b, None), self.buf("near_first", 1, j))

    def own(self, j):
        self.take(4 * j + 2, self.buf("near_first", 0, j))
        self.take(4 * j + 3, self.buf("near_first", 1, j))
        self.add(self.ref(self.a, self.dest(j), None), self.buf("near_first", 0, j), self.buf("near_first", 1, j))

    def second_far(self):
        b = shifted(self.b, 2)
        self.put(16, self.second, 1, self.ref(self.a, b, 0), self.buf("far_second", 0, 0))
        self.put(17, self.second, -1, self.ref(self.a, b, 1), self.buf("far_second", 1, 0))

    def second_up(self):
        b = shifted(self.b, 1)
        self.take(16, self.buf("far_second", 0, 0))
        self.add(self.ref(self.a, b, 0), self.buf("far_second", 0, 0))
        self.put(18, self.second, 1, self.ref(self.a, b, None), self.buf("near_second", 0, 0))

    def second_down(self):
        b = shifted(self.b, -1)
        self.take(17, self.buf("far_second", 1, 0))
        self.add(self.ref(self.a, b, 1), self.buf("far_second", 1, 0))
        self.put(19, self.second, -1, self.ref(self.a, b, None), self.buf("near_second", 1, 0))

    def total(self):
        self.take(18, self.buf("near_second", 0, 0))
        self.take(19, self.buf("near_second", 1, 0))
        total = self.ref(self.a, self.b, None)[...].astype(jnp.float32)
        total = total + self.buf("near_second", 0, 0)[...].astype(jnp.float32)
        return total + self.buf("near_second", 1, 0)[...].astype(jnp.float32)

    def finish(self):
        for copy in self.sent:
            copy.wait_send()


def layer_kernel(
    queries, keys, values, documents, query_gain, key_gain, cosines, sines,
    out_w, residuals, norm_gains, up_w, down_w, mixed,
    x_all, up_all, down_all, sums, theirs, stream, hidden, squared, squares,
    hidden_early, docs, doc_column, q_gain, k_gain, gains, send_sems, recv_sems, local_sems, free_sem,
):
    z, x, y, c = (lax.axis_index(n) for n in ("z", "x", "y", "c"))
    other = 1 - c
    sp = z * N + x
    tp = y * 2 + c
    plane = [
        {"z": shifted(z, dz), "x": shifted(x, dx)} for dz in range(N) for dx in range(N) if dz or dx
    ]
    group = [{"y": shifted(y, dy), "c": cc} for dy in range(N) for cc in (c, other) if dy or cc is other]
    wait = barrier_with(plane + group)

    def kv_place(zz, xx, start, rows):
        return sums.at[1, zz, xx, pl.ds(start, rows), :]

    def att_slot(t, part):
        rows = pl.ds(0, TOK) if part is None else pl.ds(part * HALF, HALF)
        return sums.at[0, lax.div(t, 4), lax.rem(t, 4), rows, pl.ds(0, 256)]

    def col_slot(t, start=0, rows=256):
        return theirs.at[lax.div(t, 4), lax.rem(t, 4), pl.ds(start, rows), :]

    def thousand(index):
        return pl.ds(pl.multiple_of(index * TOK, TOK), TOK)

    q_in = theirs.at[2, 0, :, pl.ds(0, 2 * HD)]
    k_in = theirs.at[2, 1, :, pl.ds(0, HD)]
    v_in = theirs.at[2, 2, :, pl.ds(0, HD)]
    q_rot = theirs.at[2, 3]
    residual = theirs.at[3, 0]
    cosine = stream.at[:, pl.ds(2 * HD, HD)]
    sine = stream.at[:, pl.ds(3 * HD, HD)]

    def local(i, src, dst):
        copy = pltpu.make_async_copy(src, dst, local_sems.at[i])
        copy.start()
        return copy

    first = [
        local(0, keys, k_in),
        local(1, values, v_in),
        local(2, cosines, cosine),
        local(3, sines, sine),
        local(4, key_gain, k_gain),
        local(5, documents, docs.at[sp]),
    ]
    second = [local(6, queries, q_in), local(7, query_gain, q_gain)]
    third = [
        local(8, residuals, residual),
        local(9, norm_gains, gains),
        local(10, out_w.at[:, thousand(tp)], col_slot(tp)),
    ]
    fourth = [
        local(11, up_w.at[:, thousand(x)], up_all.at[z, x]),
        local(12, down_w.at[thousand(x), :], down_all.at[z, x]),
    ]
    for copy in first:
        copy.wait()
    mine = kv_place(z, x, 0, 2 * HD)
    turned = jnp.transpose(rotated(k_in[...], k_gain[...], cosine[...], sine[...]).astype(jnp.float32))
    mine[HD:, :] = turned.astype(jnp.bfloat16)
    for i in range(TOK // HD):
        mine[:HD, i * HD : (i + 1) * HD] = v_in[i * HD : (i + 1) * HD, :]

    def mark(zz, xx):
        row = lax.broadcasted_iota(jnp.int32, (HD, TOK), 0)
        hot = jnp.where(row == docs[zz * N + xx], key_mark, 0.0)
        sums[1, zz, xx, 2 * HD : 3 * HD, :] = hot.astype(jnp.bfloat16)

    mark(z, x)
    column = jnp.broadcast_to(docs[sp].astype(jnp.float32), (HD, TOK))
    doc_column[...] = jnp.transpose(column).astype(jnp.int32)
    wait()

    kvs = TorusGather("x", "z", lambda a, b, s, r: kv_place(b, a, s, r), 0, 2 * HD, send_sems, recv_sems, 0)
    ups_across = Exchange(
        "x",
        lambda to, s, r: up_w.at[pl.ds(s, r), thousand(to)],
        lambda who, s, r: up_all.at[z, who, pl.ds(s, r), :],
        lambda i: squared.at[0, pl.ds(128 * i, 128), :],
        256, send_sems, recv_sems, 20,
    )
    downs_across = Exchange(
        "x",
        lambda to, s, r: down_w.at[pl.ds(pl.multiple_of(to * TOK + s, HALF), r), :],
        lambda who, s, r: down_all.at[z, who, pl.ds(s, r), :],
        lambda i: squared.at[1, pl.ds(256 * i, 256), pl.ds(0, 256)],
        512, send_sems, recv_sems, 26,
    )
    columns = []
    for i, cc in enumerate((c, other)):
        ex = Exchange(
            "y",
            lambda to, s, r, cc=cc: out_w.at[pl.ds(s, r), thousand(to * 2 + cc)],
            lambda who, s, r: col_slot(who * 2 + c, s, r),
            lambda k, i=i: squared.at[2, pl.ds(128 * (2 * i + k), 128), :],
            256, send_sems, recv_sems, 32 + 6 * i, {"c": cc},
        )
        ex.landed = lambda who, s, r, cc=cc: col_slot(who * 2 + cc, s, r)
        columns.append(ex)
    kvs.begin()
    doc_copies = [
        send(docs.at[sp], docs.at[sp], send_sems.at[45 + i], recv_sems.at[45 + i], peer)
        for i, peer in enumerate(plane)
    ]
    for ex in columns:
        ex.begin()
    twin = send(
        out_w.at[:, thousand(y * 2 + other)], col_slot(tp), send_sems.at[44], recv_sems.at[44], {"c": other}
    )

    for copy in second:
        copy.wait()
    lane = lax.broadcasted_iota(jnp.int32, (TOK, HD), 1)
    hot = jnp.where(lane == doc_column[...], query_mark, 0.0).astype(jnp.bfloat16)
    for h in range(2):
        turn = rotated(q_in[:, h * HD : (h + 1) * HD], q_gain[...], cosine[...], sine[...])
        for t in range(2):
            rows, part = slice(h * HALF, (h + 1) * HALF), slice(t * HALF, (t + 1) * HALF)
            q_rot[rows, 2 * t * HD : (2 * t + 1) * HD] = turn[part]
            q_rot[rows, (2 * t + 1) * HD : (2 * t + 2) * HD] = hot[part]
    hidden[:, :HD] = jnp.zeros((2 * TOK, HD), jnp.float32)
    hidden[:, HD : 2 * HD] = jnp.full((2 * TOK, HD), masked_score, jnp.float32)
    hidden[:, 2 * HD : 3 * HD] = jnp.zeros((2 * TOK, HD), jnp.float32)
    scale = HD ** (-0.5) * 1.4426950408889634

    def attend(count, which):
        @pl.loop(0, 2)
        def _(t):
            rows = pl.ds(pl.multiple_of(t * TOK, TOK), TOK)
            q = q_rot[:, pl.ds(pl.multiple_of(t * HALF, HALF), HALF)]
            cuts = [slice(i * HD, (i + 1) * HD) for i in range(4)]

            def step(i, carry):
                top, total, weighted = carry
                zz, xx = which(i)
                packed = sums[1, zz, xx, :HD, :]
                v = jnp.concatenate([packed[:, cut] for cut in cuts], axis=0)
                s = jnp.dot(q, sums[1, zz, xx, HD : 3 * HD, :], preferred_element_type=jnp.float32)
                s = [s[:, cut] for cut in cuts]
                most = jnp.maximum(jnp.maximum(s[0], s[1]), jnp.maximum(s[2], s[3]))
                new_top = jnp.maximum(top, jnp.max(most, axis=-1, keepdims=True))
                p = [jnp.exp2((part - new_top) * scale) for part in s]
                fade = jnp.exp2((top - new_top) * scale)
                total = total * fade + ((p[0] + p[1]) + (p[2] + p[3]))
                low = jnp.concatenate([part.astype(jnp.bfloat16) for part in p], axis=1)
                weighted = weighted * fade + jnp.dot(low, v, preferred_element_type=jnp.float32)
                return new_top, total, weighted

            start = (hidden[rows, cuts[1]], hidden[rows, cuts[2]], hidden[rows, cuts[0]])
            top, total, weighted = lax.fori_loop(0, count, step, start)
            hidden[rows, cuts[1]] = top
            hidden[rows, cuts[2]] = total
            hidden[rows, cuts[0]] = weighted

    attend(1, lambda i: (z, x))
    kvs.near()
    kvs.far()
    ups_across.begin()
    downs_across.begin()
    for i, peer in enumerate(plane):
        dz, dx = divmod(i + 1, N)
        arrived(
            docs.at[shifted(z, -dz) * N + shifted(x, -dx)], send_sems.at[45 + i], recv_sems.at[45 + i], {"z": z}
        )

    @pl.loop(1, 16)
    def _(i):
        mark(lax.rem(z + lax.div(i, N), N), lax.rem(x + i, N))

    attend(3, lambda i: (z, lax.rem(x + 1 + i, N)))
    kvs.pass_on(0)
    kvs.pass_on(1)
    for ex in columns:
        ex.pass_on()
    attend(4, lambda i: (lax.rem(z + 1 + 2 * lax.rem(i, 2), N), lax.rem(x + N - lax.div(i, 2), N)))
    kvs.pass_on(2)
    kvs.pass_on(3)
    ups_across.pass_on()
    downs_across.pass_on()
    attend(4, lambda i: (lax.rem(z + 1 + 2 * lax.rem(i, 2), N), lax.rem(x + 1 + lax.div(i, 2), N)))
    kvs.last(0)
    kvs.last(1)
    attend(2, lambda i: (lax.rem(z + 2, N), lax.rem(x + N - i, N)))
    kvs.last(2)
    kvs.last(3)
    def half_of(ref, z_at, part):
        at = ref.at[z_at]
        return at if part is None else at.at[pl.ds(2 * part, 2)]

    ups = RingGather(
        "z", lambda who, part: half_of(up_all, who, part), up_all.at[z], send_sems, recv_sems, 68
    )
    downs = RingGather(
        "z", lambda who, part: half_of(down_all, who, part), down_all.at[z], send_sems, recv_sems, 72
    )
    for copy in fourth:
        copy.wait()
    ups_across.last()
    ups.begin()
    attend(2, lambda i: (lax.rem(z + 2, N), lax.rem(x + 1 + i, N)))

    att = att_slot(tp, None)
    for t in range(2):
        for h in range(2):
            rows = slice(t * TOK + h * HALF, t * TOK + (h + 1) * HALF)
            total = jnp.sum(hidden[rows, 2 * HD : 3 * HD], axis=-1, keepdims=True)
            att[t * HALF : (t + 1) * HALF, h * HD : (h + 1) * HD] = (hidden[rows, :HD] / total).astype(jnp.bfloat16)

    handed = []

    def hand(k, src, dst):
        handed.append(send(src, dst, send_sems.at[k], recv_sems.at[k], {"c": other}))

    def taken(k, dst):
        arrived(dst, send_sems.at[k], recv_sems.at[k], {"c": c})

    heads = RingGather("y", lambda who, part: att_slot(who * 2 + c, part), att, send_sems, recv_sems, 60)
    heads.begin()
    hand(64, att, att)

    for copy in third:
        copy.wait()
    for ex in columns:
        ex.target = ex.landed
        ex.last()
    arrived(col_slot(y * 2 + other), send_sems.at[44], recv_sems.at[44], {"c": c})

    def project(t):
        part = jnp.dot(att_slot(t, None)[...], col_slot(t)[...], preferred_element_type=jnp.float32)
        stream[...] += part.astype(jnp.bfloat16).astype(jnp.float32)

    y_low, y_high, y_far = shifted(y, -1), shifted(y, 1), shifted(y, 2)
    stream[...] = residual[...].astype(jnp.float32)
    project(tp)
    heads.low()
    hand(65, att_slot(y_low * 2 + c, None), att_slot(y_low * 2 + c, None))
    heads.high()
    hand(66, att_slot(y_high * 2 + c, None), att_slot(y_high * 2 + c, None))
    taken(64, att_slot(y * 2 + other, None))
    project(y * 2 + other)
    project(y_low * 2 + c)
    project(y_high * 2 + c)
    heads.far()
    hand(67, att_slot(y_far * 2 + c, None), att_slot(y_far * 2 + c, None))
    taken(65, att_slot(y_low * 2 + other, None))
    project(y_low * 2 + other)
    taken(66, att_slot(y_high * 2 + other, None))
    project(y_high * 2 + other)
    project(y_far * 2 + c)
    taken(67, att_slot(y_far * 2 + other, None))
    project(y_far * 2 + other)

    whole = stream[...]
    partial = jnp.sum(whole * whole, axis=-1, keepdims=True)
    squares[tp] = jnp.transpose(jnp.broadcast_to(partial, (TOK, HD)))[:8]
    square_copies = [
        send(squares.at[tp], squares.at[tp], send_sems.at[76 + i], recv_sems.at[76 + i], peer)
        for i, peer in enumerate(group)
    ]
    downs_across.last()
    for done in (heads, kvs, ups_across, downs_across, *columns):
        done.finish()
    for copy in (*handed, *doc_copies, twin):
        copy.wait_send()
    handed.clear()
    i = 0
    for dy in range(N):
        for cc in (c, other):
            if dy or cc is other:
                arrived(squares.at[shifted(y, -dy) * 2 + cc], send_sems.at[76 + i], recv_sems.at[76 + i], {"c": c})
                i += 1
    full = squares[0]
    for t in range(1, 8):
        full = full + squares[t]
    full = jnp.transpose(jnp.broadcast_to(full[:1], (HD, TOK)))
    inverse = lax.rsqrt(full[:, :1] / D + norm_eps)
    x_all[x, tp] = (stream[...] * inverse * gains[tp]).astype(jnp.bfloat16)

    def place(xx, yy, start, rows):
        return x_all.at[xx, yy * 2 + c, pl.ds(start, rows), :]

    gathers = [
        TorusGather("y", "x", lambda a, b, s, r: place(b, a, s, r), 0, HALF, send_sems, recv_sems, 83),
        TorusGather("x", "y", place, HALF, HALF, send_sems, recv_sems, 103),
    ]

    def share(n, j, i):
        g = gathers[n]
        ref = g.ref(g.order(j), shifted(g.b, (0, -1, 1, 2)[i]), None)
        hand(123 + 16 * n + 4 * j + i, ref, ref)

    def shared(n, j, i):
        g = gathers[n]
        a, b = g.order(j), shifted(g.b, (0, -1, 1, 2)[i])
        xx, yy = (b, a) if n == 0 else (a, b)
        taken(123 + 16 * n + 4 * j + i, x_all.at[xx, yy * 2 + other, pl.ds(n * HALF, HALF), :])

    def weight(t):
        return up_all[lax.div(t, 2), pl.ds(2 * lax.rem(t, 2), 2)].reshape(TOK, TOK)

    def square(value):
        positive = jnp.maximum(value, 0.0)
        return (positive * positive).astype(jnp.bfloat16)

    def early(blocks, first, count, step, clear, store):
        rows = HALF * len(blocks)
        acc = hidden_early.at[pl.ds(0, rows)]
        if clear:
            acc[...] = jnp.zeros_like(acc)

        @pl.loop(0, count)
        def _(i):
            t = lax.rem(first + step * i, 8)
            parts = [x_all[xx, t, :HALF, :] for xx in blocks]
            part = parts[0] if len(parts) == 1 else jnp.concatenate(parts, axis=0)
            acc[...] += jnp.dot(part, weight(t), preferred_element_type=jnp.float32)

        if store:
            for i, xx in enumerate(blocks):
                squared[xx, :HALF, :] = square(hidden_early[i * HALF : (i + 1) * HALF, :])

    def late(first, count, step):
        @pl.loop(0, count)
        def _(i):
            t = lax.rem(first + step * i, 8)
            rows = x_all[:, t, HALF:, :].reshape(N * HALF, TOK)
            hidden[...] += jnp.dot(rows, weight(t), preferred_element_type=jnp.float32)

    for g in gathers:
        g.begin()
    for n in range(2):
        share(n, 0, 0)
    hidden[...] = jnp.zeros_like(hidden)
    for n, g in enumerate(gathers):
        g.near()
        share(n, 1, 0)
        share(n, 2, 0)
    ups.low()
    ups.high()
    downs.begin()
    for n, g in enumerate(gathers):
        g.far()
        share(n, 3, 0)
    ups.far()
    for j in range(N):
        for n in range(2):
            shared(n, j, 0)
    early([x], 0, 8, 1, True, True)
    for j in range(N):
        for n, g in enumerate(gathers):
            g.pass_on(j)
            share(n, j, 1)
            share(n, j, 2)
    late(2 * (y + 3) + c, 3, 2)
    late(2 * y + other, 1, 2)
    for j in range(N):
        for i in (1, 2):
            for n in range(2):
                shared(n, j, i)
    late(2 * (y + 3) + other, 2, 4)
    sides = [shifted(x, -1), shifted(x, 1)]
    early(sides, 0, 4, 1, True, False)
    for j in range(2):
        for n, g in enumerate(gathers):
            g.last(j)
            share(n, j, 3)
    early(sides, 4, 4, 1, False, True)
    for j in range(2, N):
        for n, g in enumerate(gathers):
            g.last(j)
            share(n, j, 3)
    downs.low()
    downs.high()
    opposite = [shifted(x, 2)]
    late(2 * (y + 2) + c, 1, 2)
    early(opposite, c, 4, 2, True, False)
    for j in range(N):
        for n in range(2):
            shared(n, j, 3)
    early(opposite, other, 4, 2, False, True)
    late(2 * (y + 2) + other, 1, 2)
    for g in gathers:
        g.finish()
    for copy in handed:
        copy.wait_send()
    handed.clear()
    for peer in ({"x": shifted(x, 1)}, {"x": shifted(x, -1)}, {"y": shifted(y, 1)}, {"y": shifted(y, -1)}):
        pl.semaphore_signal(free_sem, inc=1, device_id=peer, device_id_type=MESH)

    @pl.loop(0, N)
    def _(xx):
        rows = pl.ds(pl.multiple_of(xx * HALF, HALF), HALF)
        squared[xx, HALF:, :] = square(hidden[rows, :])

    downs.far()

    def feed(i, xx):
        def columns_of(cc):
            @pl.loop(0, N)
            def _(yy):
                pair = [down_all[yy, 2 * cc + part] for part in range(2)]
                sums[cc, xx, yy] = jnp.dot(
                    squared[xx], jnp.concatenate(pair, axis=1), preferred_element_type=jnp.float32
                ).astype(jnp.bfloat16)

        columns_of(other)
        hand(155 + i, sums.at[other, xx], theirs.at[xx])
        columns_of(c)

    def joined(i, xx):
        taken(155 + i, theirs.at[xx])

        @pl.loop(0, N)
        def _(yy):
            TorusReduce.add(sums.at[c, xx, yy], theirs.at[xx, yy])

    def sum_place(xx, yy, start, rows):
        return sums.at[c, xx, yy, pl.ds(start, rows), :]

    def bufs(n):
        def buf(kind, way, j):
            if kind == "near_first":
                return x_all.at[n, 4 * way + j, pl.ds(0, HALF), :]
            if kind == "far_first":
                return x_all.at[n, 4 * way + j, pl.ds(HALF, HALF // 2), :]
            if kind == "near_second":
                return x_all.at[2, 2 * n + way, pl.ds(0, HALF), :]
            return x_all.at[2, 2 * n + way, pl.ds(HALF, HALF // 2), :]

        return buf

    rows_x = TorusReduce("x", "y", sum_place, 0, HALF, bufs(0), send_sems, recv_sems, 159)
    rows_y = TorusReduce(
        "y", "x", lambda a, b, s, r: sum_place(b, a, s, r), HALF, HALF, bufs(1), send_sems, recv_sems, 179
    )
    blocks = [rows_y.dest(j) for j in range(N)]
    feed(0, blocks[0])
    feed(1, blocks[1])
    pl.semaphore_wait(free_sem, 4)
    joined(0, blocks[0])
    for j in range(N):
        rows_x.far(j)
    rows_y.far(0)
    feed(2, blocks[2])
    joined(1, blocks[1])
    rows_y.far(1)
    rows_y.up(0)
    rows_y.down(0)
    feed(3, blocks[3])
    joined(2, blocks[2])
    rows_y.far(2)
    rows_y.up(1)
    rows_y.down(1)
    for j in range(2):
        rows_x.up(j)
        rows_x.down(j)
    joined(3, blocks[3])
    rows_y.far(3)
    for j in range(2, N):
        rows_x.up(j)
        rows_x.down(j)
        rows_y.up(j)
        rows_y.down(j)
    for j in range(N):
        for r in (rows_x, rows_y):
            r.own(j)
            if j == 0:
                r.second_far()
            if j == 1:
                r.second_up()
            if j == 2:
                r.second_down()
    mixed[:HALF, :] = (stream[:HALF, :] + rows_x.total()).astype(jnp.bfloat16)
    mixed[HALF:, :] = (stream[HALF:, :] + rows_y.total()).astype(jnp.bfloat16)
    for done in (ups, downs, rows_x, rows_y):
        done.finish()
    for copy in (*handed, *square_copies):
        copy.wait_send()


def body(
    queries, keys, values, documents, query_gain, key_gain, residual, out_weight, norm_gain, up_weight, down_weight
):
    bf, f32 = jnp.bfloat16, jnp.float32
    cosine, sine = tables(lax.axis_index(("z", "x")))
    return pl.pallas_call(
        layer_kernel,
        out_shape=jax.ShapeDtypeStruct((TOK, TOK), bf),
        in_specs=[ANY] * 13,
        out_specs=VMEM,
        scratch_shapes=[
            pltpu.VMEM((N, 8, TOK, TOK), bf),
            pltpu.VMEM((N, N, 256, TOK), bf),
            pltpu.VMEM((N, N, TOK, 256), bf),
            pltpu.VMEM((2, N, N, TOK, TOK), bf),
            pltpu.VMEM((N, N, TOK, TOK), bf),
            pltpu.VMEM((TOK, TOK), f32),
            pltpu.VMEM((N * HALF, TOK), f32),
            pltpu.VMEM((N, TOK, TOK), bf),
            pltpu.VMEM((8, 8, TOK), f32),
            pltpu.VMEM((TOK, TOK), f32),
            pltpu.VMEM((16, 1, TOK), jnp.int32),
            pltpu.VMEM((TOK, HD), jnp.int32),
            pltpu.VMEM((1, HD), f32),
            pltpu.VMEM((1, HD), f32),
            pltpu.VMEM((8, 1, TOK), f32),
            pltpu.SemaphoreType.DMA((199,)),
            pltpu.SemaphoreType.DMA((199,)),
            pltpu.SemaphoreType.DMA((13,)),
            pltpu.SemaphoreType.REGULAR,
        ],
        compiler_params=pltpu.CompilerParams(
            collective_id=0, has_side_effects=True, vmem_limit_bytes=67043328
        ),
        name="layer",
    )(
        queries, keys, values, documents.reshape(1, TOK), query_gain.reshape(1, HD), key_gain.reshape(1, HD),
        cosine, sine, out_weight, residual, norm_gain.reshape(8, 1, TOK), up_weight, down_weight,
    )


def solution(mesh):
    split = Mesh(mesh.devices.reshape(N, N, N, 2), ("z", "x", "y", "c"))
    sp, tp = ("z", "x"), ("y", "c")
    return jax.shard_map(
        body,
        mesh=split,
        in_specs=(
            P(sp, tp), P(sp, tp), P(sp, tp), P(sp), P(), P(), P(sp, tp), P(tp, None), P(), P(sp, tp), P(tp, sp),
        ),
        out_specs=P(sp, tp),
        check_vma=False,
    )
```

time: 240 us -> 188 us (0.78)
  Pallas kernels: 223 us -> 184 us
  local copies, waits for them, and re-layouts: 13.9 us -> 1.87 us
    pallas_call x3 -> x1, Pallas kernels: 223 us -> 184 us  [body(): pl.pallas_call(layer_kernel, out_shape=jax.ShapeDtypeStruct((TOK, TOK), b...]
    unnamed x27 -> x1, local copies, waits for them, and re-layouts: 13.1 us -> 1.87 us
where the time goes in v2:
time: 188 us; the launch traced here: 187 us
  Pallas kernels  184 us (98%)
    pallas_call x1, Pallas kernels, body(): pl.pallas_call(layer_kernel, out_shape=jax.ShapeDtypeStruct((TOK, TOK), b...  184 us

profile of v2, /device:TPU:0, one launch (start us, length us, event | category | flops | bytes accessed | tf_op | source)
XLA Modules:
  0.0 187.5 jit_solution(14446568033605014896)
XLA Ops:
  0.0 1.8 sine_multiply_fusion
  1.9 183.7 %layer.1 = bf16[512,512]{1,0:T(8,128)(2,1)} custom-call(bf16[512,256]{1,0:T(8,128)(2,1)} %queries.1, bf16[512,128]{1,0:T(8,128)(2,1)} %keys.1, bf16[512,128]{1,0:T(8,128)(2,1)} %values.1, s32[1,512]{1,0:T(1,128)} %bitcast.5, f32[1,128]{1,0:T(1,128)} %bitcast.6, f32[1,128]{1,0:T(1,128)} %bitcast.7, f32[512,128]{1,0:T(8,128)} %get-tuple-element.6.cosines, ...), custom_call_target="tpu_custom_call" | custom-call | tf_op jit(solution)/shard_map/layer/pallas_call | solution.py:826
  185.6 1.9 copy.13
  (3 shorter events, 0.0 us)

commit v3 on v2

--- a/solution.py
+++ b/solution.py
@@ -92,6 +92,11 @@
     def begin(self):
         self.put(0, self.first, 1, self.a, self.b, None)
         self.put(1, self.first, -1, self.a, self.b, None)
+
+    def follow(self):
+        for copy in self.sent:
+            copy.wait_send()
+        self.sent.clear()
         self.spread(0)
 
     def near(self):
@@ -438,6 +443,7 @@
         ex.landed = lambda who, s, r, cc=cc: col_slot(who * 2 + cc, s, r)
         columns.append(ex)
     kvs.begin()
+    kvs.spread(0)
     doc_copies = [
         send(docs.at[sp], docs.at[sp], send_sems.at[45 + i], recv_sems.at[45 + i], peer)
         for i, peer in enumerate(plane)
@@ -580,6 +586,7 @@
     project(y * 2 + other)
     project(y_low * 2 + c)
     project(y_high * 2 + c)
+    downs_across.last()
     heads.far()
     hand(67, att_slot(y_far * 2 + c, None), att_slot(y_far * 2 + c, None))
     taken(65, att_slot(y_low * 2 + other, None))
@@ -597,7 +604,6 @@
         send(squares.at[tp], squares.at[tp], send_sems.at[76 + i], recv_sems.at[76 + i], peer)
         for i, peer in enumerate(group)
     ]
-    downs_across.last()
     for done in (heads, kvs, ups_across, downs_across, *columns):
         done.finish()
     for copy in (*handed, *doc_copies, twin):
@@ -670,22 +676,25 @@
         g.begin()
     for n in range(2):
         share(n, 0, 0)
+    ups.low()
+    ups.high()
+    downs.begin()
+    for g in gathers:
+        g.follow()
     hidden[...] = jnp.zeros_like(hidden)
     for n, g in enumerate(gathers):
         g.near()
         share(n, 1, 0)
         share(n, 2, 0)
-    ups.low()
-    ups.high()
-    downs.begin()
     for n, g in enumerate(gathers):
         g.far()
         share(n, 3, 0)
     ups.far()
-    for j in range(N):
-        for n in range(2):
+    for n in range(2):
+        for j in range(N):
             shared(n, j, 0)
-    early([x], 0, 8, 1, True, True)
+        if n == 0:
+            early([x], 0, 8, 1, True, True)
     for j in range(N):
         for n, g in enumerate(gathers):
             g.pass_on(j)
@@ -698,27 +707,28 @@
             for n in range(2):
                 shared(n, j, i)
     late(2 * (y + 3) + other, 2, 4)
+    downs.low()
+    downs.high()
     sides = [shifted(x, -1), shifted(x, 1)]
     early(sides, 0, 4, 1, True, False)
-    for j in range(2):
+    for j in range(N):
         for n, g in enumerate(gathers):
             g.last(j)
             share(n, j, 3)
     early(sides, 4, 4, 1, False, True)
-    for j in range(2, N):
-        for n, g in enumerate(gathers):
-            g.last(j)
-            share(n, j, 3)
-    downs.low()
-    downs.high()
     opposite = [shifted(x, 2)]
     late(2 * (y + 2) + c, 1, 2)
     early(opposite, c, 4, 2, True, False)
-    for j in range(N):
-        for n in range(2):
+    for n in range(2):
+        for j in range(N):
             shared(n, j, 3)
     early(opposite, other, 4, 2, False, True)
     late(2 * (y + 2) + other, 1, 2)
+    @pl.loop(0, N)
+    def _(xx):
+        rows = pl.ds(pl.multiple_of(xx * HALF, HALF), HALF)
+        squared[xx, HALF:, :] = square(hidden[rows, :])
+
     for g in gathers:
         g.finish()
     for copy in handed:
@@ -727,28 +737,28 @@
     for peer in ({"x": shifted(x, 1)}, {"x": shifted(x, -1)}, {"y": shifted(y, 1)}, {"y": shifted(y, -1)}):
         pl.semaphore_signal(free_sem, inc=1, device_id=peer, device_id_type=MESH)
 
-    @pl.loop(0, N)
-    def _(xx):
-        rows = pl.ds(pl.multiple_of(xx * HALF, HALF), HALF)
-        squared[xx, HALF:, :] = square(hidden[rows, :])
-
-    downs.far()
-
-    def feed(i, xx):
-        def columns_of(cc):
-            @pl.loop(0, N)
-            def _(yy):
-                pair = [down_all[yy, 2 * cc + part] for part in range(2)]
-                sums[cc, xx, yy] = jnp.dot(
-                    squared[xx], jnp.concatenate(pair, axis=1), preferred_element_type=jnp.float32
-                ).astype(jnp.bfloat16)
-
-        columns_of(other)
-        hand(155 + i, sums.at[other, xx], theirs.at[xx])
-        columns_of(c)
+    def column(cc, xx, yy):
+        pair = [down_all[yy, 2 * cc + part] for part in range(2)]
+        sums[cc, xx, yy] = jnp.dot(
+            squared[xx], jnp.concatenate(pair, axis=1), preferred_element_type=jnp.float32
+        ).astype(jnp.bfloat16)
+
+    def near_columns(cc, xx):
+        @pl.loop(0, N - 1)
+        def _(i):
+            column(cc, xx, lax.rem(z + 3 + i, N))
+
+    def far_column(cc, xx):
+        column(cc, xx, shifted(z, 2))
+
+    def hand_on(i, xx, offsets):
+        for k in offsets:
+            yy = shifted(z, k)
+            hand((155, 199, 203, 207)[i] + k % N, sums.at[other, xx, yy], theirs.at[xx, yy])
 
     def joined(i, xx):
-        taken(155 + i, theirs.at[xx])
+        for k in range(N):
+            taken((155, 199, 203, 207)[i] + k, theirs.at[xx, shifted(z, k)])
 
         @pl.loop(0, N)
         def _(yy):
@@ -774,42 +784,67 @@
         "y", "x", lambda a, b, s, r: sum_place(b, a, s, r), HALF, HALF, bufs(1), send_sems, recv_sems, 179
     )
     blocks = [rows_y.dest(j) for j in range(N)]
-    feed(0, blocks[0])
-    feed(1, blocks[1])
+    for i in range(2):
+        near_columns(other, blocks[i])
+        hand_on(i, blocks[i], (-1, 0, 1))
+    near_columns(c, blocks[0])
+    downs.far()
+    far_column(other, blocks[0])
+    hand_on(0, blocks[0], (2,))
+    far_column(c, blocks[0])
+    far_column(other, blocks[1])
+    hand_on(1, blocks[1], (2,))
     pl.semaphore_wait(free_sem, 4)
     joined(0, blocks[0])
     for j in range(N):
         rows_x.far(j)
     rows_y.far(0)
-    feed(2, blocks[2])
+    near_columns(c, blocks[1])
+    far_column(c, blocks[1])
     joined(1, blocks[1])
     rows_y.far(1)
+    near_columns(other, blocks[2])
+    far_column(other, blocks[2])
+    hand_on(2, blocks[2], (-1, 0, 1, 2))
     rows_y.up(0)
     rows_y.down(0)
-    feed(3, blocks[3])
+    near_columns(c, blocks[2])
+    far_column(c, blocks[2])
+    near_columns(other, blocks[3])
+    far_column(other, blocks[3])
+    hand_on(3, blocks[3], (-1, 0, 1, 2))
     joined(2, blocks[2])
     rows_y.far(2)
     rows_y.up(1)
     rows_y.down(1)
+    near_columns(c, blocks[3])
+    far_column(c, blocks[3])
+    joined(3, blocks[3])
+    rows_y.far(3)
     for j in range(2):
         rows_x.up(j)
         rows_x.down(j)
-    joined(3, blocks[3])
-    rows_y.far(3)
+    rows_y.up(2)
+    rows_y.down(2)
+    rows_y.own(0)
+    rows_y.second_far()
     for j in range(2, N):
         rows_x.up(j)
         rows_x.down(j)
-        rows_y.up(j)
-        rows_y.down(j)
-    for j in range(N):
-        for r in (rows_x, rows_y):
-            r.own(j)
-            if j == 0:
-                r.second_far()
-            if j == 1:
-                r.second_up()
-            if j == 2:
-                r.second_down()
+    rows_y.up(3)
+    rows_y.down(3)
+    rows_y.own(1)
+    rows_y.second_up()
+    rows_x.own(0)
+    rows_x.second_far()
+    rows_x.own(1)
+    rows_y.own(2)
+    rows_y.second_down()
+    rows_x.second_up()
+    rows_x.own(2)
+    rows_x.second_down()
+    rows_y.own(3)
+    rows_x.own(3)
     mixed[:HALF, :] = (stream[:HALF, :] + rows_x.total()).astype(jnp.bfloat16)
     mixed[HALF:, :] = (stream[HALF:, :] + rows_y.total()).astype(jnp.bfloat16)
     for done in (ups, downs, rows_x, rows_y):
@@ -844,8 +879,8 @@
             pltpu.VMEM((1, HD), f32),
             pltpu.VMEM((1, HD), f32),
             pltpu.VMEM((8, 1, TOK), f32),
-            pltpu.SemaphoreType.DMA((199,)),
-            pltpu.SemaphoreType.DMA((199,)),
+            pltpu.SemaphoreType.DMA((211,)),
+            pltpu.SemaphoreType.DMA((211,)),
             pltpu.SemaphoreType.DMA((13,)),
             pltpu.SemaphoreType.REGULAR,
         ],

time: 188 us -> 181 us (0.963)
  Pallas kernels: 184 us -> 177 us
    pallas_call x1, Pallas kernels: 184 us -> 177 us  [body(): pl.pallas_call(layer_kernel, out_shape=jax.ShapeDtypeStruct((TOK, TOK), b...]
where the time goes in v3:
time: 181 us
  Pallas kernels  177 us (98%)
  other arithmetic  1.88 us (1%)
  local copies, waits for them, and re-layouts  1.87 us (1%)
    pallas_call x1, Pallas kernels, body(): pl.pallas_call(layer_kernel, out_shape=jax.ShapeDtypeStruct((TOK, TOK), b...  177 us

profile of v3, /device:TPU:0, one launch (start us, length us, event | category | flops | bytes accessed | tf_op | source)
XLA Modules:
  0.0 180.5 jit_solution(9934406678043353194)
XLA Ops:
  0.0 1.8 %sine_multiply_fusion = (f32[512,128]{1,0:T(8,128)}, f32[512,128]{1,0:T(8,128)}) fusion(f32[128]{0:T(128)S(1)} %get-tuple-element.9, f32[128]{0:T(128)S(1)} %get-tuple-element.10, s32[512]{0:T(512)S(1)} %get-tuple-element.7, s32[512]{0:T(512)S(1)} %get-tuple-element.8, pred[128]{0:T(512)(128)(4,1)S(1)} %iota_compare_fusion), kind=kLoop, calls=%fused_computation | loop fusion | flops 262144 | bytes 529536 | tf_op jit(solution)/shard_map/mul | solution.py:209
  1.9 176.8 %layer.1 = bf16[512,512]{1,0:T(8,128)(2,1)} custom-call(bf16[512,256]{1,0:T(8,128)(2,1)} %queries.1, bf16[512,128]{1,0:T(8,128)(2,1)} %keys.1, bf16[512,128]{1,0:T(8,128)(2,1)} %values.1, s32[1,512]{1,0:T(1,128)} %bitcast.5, f32[1,128]{1,0:T(1,128)} %bitcast.6, f32[1,128]{1,0:T(1,128)} %bitcast.7, f32[512,128]{1,0:T(8,128)} %get-tuple-element.6.cosines, ...), custom_call_target="tpu_custom_call" | custom-call | tf_op jit(solution)/shard_map/layer/pallas_call | solution.py:861
  178.7 1.9 %copy.13 = bf16[512,512]{1,0:T(8,128)(2,1)} copy(bf16[512,512]{1,0:T(8,128)(2,1)} %layer.1) | data formatting | bytes 1048576
  (3 shorter events, 0.0 us)

commit v4 on v3

--- a/solution.py
+++ b/solution.py
@@ -1,6 +1,7 @@
 import functools
 import jax
 import jax.numpy as jnp
+import numpy as np
 from jax import lax
 from jax.experimental import pallas as pl
 from jax.experimental.pallas import tpu as pltpu
@@ -196,17 +197,20 @@
     return lambda: pl.semaphore_wait(barrier, len(peers))
 
 
-def tables(sp):
-    position = sp * TOK + jnp.arange(TOK, dtype=jnp.int32)
-    lane = jnp.arange(HD, dtype=jnp.int32)
+def tables():
+    lane = np.arange(HD)
     quarter = HD // 4
-    inverse_freq = rope_base ** (-(lane % quarter).astype(jnp.float32) / quarter)
-    place = jnp.where(
-        lane[None, :] < HD // 2, (position // GRID_W)[:, None], (position % GRID_W)[:, None]
-    ).astype(jnp.float32)
-    angles = place * inverse_freq[None, :]
-    sign = jnp.where(lane % (HD // 2) < quarter, -1.0, 1.0)
-    return jnp.cos(angles), jnp.sin(angles) * sign[None, :]
+    inverse_freq = np.float32(rope_base) ** (-(lane % quarter).astype(np.float32) / np.float32(quarter))
+    sign = np.where(lane % (HD // 2) < quarter, -1.0, 1.0).astype(np.float32)
+    rows = np.arange(16 * TOK // GRID_W, dtype=np.float32)[:, None] * inverse_freq
+    columns = np.arange(GRID_W, dtype=np.float32)[:, None] * inverse_freq
+    of_row = lane < HD // 2
+
+    def table(angles, used):
+        pair = np.stack([np.cos(angles), np.sin(angles) * sign])
+        return jnp.asarray(np.where(used, pair, 0.0).astype(np.float32))
+
+    return table(rows, of_row), table(columns, ~of_row)
 
 
 class RingGather:
@@ -339,10 +343,10 @@
 
 
 def layer_kernel(
-    queries, keys, values, documents, query_gain, key_gain, cosines, sines,
+    queries, keys, values, documents, query_gain, key_gain, row_table, column_table,
     out_w, residuals, norm_gains, up_w, down_w, mixed,
     x_all, up_all, down_all, sums, theirs, stream, hidden, squared, squares,
-    hidden_early, docs, doc_column, q_gain, k_gain, gains, send_sems, recv_sems, local_sems, free_sem,
+    hidden_early, totals, inverse, of_rows, of_columns, docs, doc_column, q_gain, k_gain, gains, send_sems, recv_sems, local_sems, free_sem,
 ):
     z, x, y, c = (lax.axis_index(n) for n in ("z", "x", "y", "c"))
     other = 1 - c
@@ -383,8 +387,8 @@
     first = [
         local(0, keys, k_in),
         local(1, values, v_in),
-        local(2, cosines, cosine),
-        local(3, sines, sine),
+        local(2, row_table.at[:, pl.ds(pl.multiple_of(sp * 8, 8), 8), :], of_rows),
+        local(3, column_table, of_columns),
         local(4, key_gain, k_gain),
         local(5, documents, docs.at[sp]),
     ]
@@ -400,6 +404,10 @@
     ]
     for copy in first:
         copy.wait()
+    for i in range(TOK // GRID_W):
+        grid_row = slice(i * GRID_W, (i + 1) * GRID_W)
+        cosine[grid_row, :] = of_rows[0, i : i + 1, :] + of_columns[0]
+        sine[grid_row, :] = of_rows[1, i : i + 1, :] + of_columns[1]
     mine = kv_place(z, x, 0, 2 * HD)
     turned = jnp.transpose(rotated(k_in[...], k_gain[...], cosine[...], sine[...]).astype(jnp.float32))
     mine[HD:, :] = turned.astype(jnp.bfloat16)
@@ -560,8 +568,17 @@
     def taken(k, dst):
         arrived(dst, send_sems.at[k], recv_sems.at[k], {"c": c})
 
-    heads = RingGather("y", lambda who, part: att_slot(who * 2 + c, part), att, send_sems, recv_sems, 60)
-    heads.begin()
+    heads_sent = []
+
+    def pass_heads(k, who, part, by):
+        ref = att_slot(who * 2 + c, part)
+        heads_sent.append(send(ref, ref, send_sems.at[k], recv_sems.at[k], {"y": shifted(y, by)}))
+
+    def take_heads(k, who, part):
+        taken(k, att_slot(who * 2 + c, part))
+
+    pass_heads(60, y, 0, 1)
+    pass_heads(61, y, 1, -1)
     hand(64, att, att)
 
     for copy in third:
@@ -577,17 +594,27 @@
 
     y_low, y_high, y_far = shifted(y, -1), shifted(y, 1), shifted(y, 2)
     stream[...] = residual[...].astype(jnp.float32)
+    for copy in heads_sent:
+        copy.wait_send()
+    heads_sent.clear()
+    pass_heads(214, y, 1, 1)
+    pass_heads(215, y, 0, -1)
     project(tp)
-    heads.low()
+    take_heads(60, y_low, 0)
+    pass_heads(62, y_low, 0, 1)
+    take_heads(61, y_high, 1)
+    pass_heads(63, y_high, 1, -1)
+    take_heads(214, y_low, 1)
     hand(65, att_slot(y_low * 2 + c, None), att_slot(y_low * 2 + c, None))
-    heads.high()
+    take_heads(215, y_high, 0)
     hand(66, att_slot(y_high * 2 + c, None), att_slot(y_high * 2 + c, None))
     taken(64, att_slot(y * 2 + other, None))
     project(y * 2 + other)
     project(y_low * 2 + c)
     project(y_high * 2 + c)
     downs_across.last()
-    heads.far()
+    take_heads(62, y_far, 0)
+    take_heads(63, y_far, 1)
     hand(67, att_slot(y_far * 2 + c, None), att_slot(y_far * 2 + c, None))
     taken(65, att_slot(y_low * 2 + other, None))
     project(y_low * 2 + other)
@@ -597,6 +624,64 @@
     taken(67, att_slot(y_far * 2 + other, None))
     project(y_far * 2 + other)
 
+    x_all[x, tp] = (stream[...] * gains[tp]).astype(jnp.bfloat16)
+
+    def place(xx, yy, start, rows):
+        return x_all.at[xx, yy * 2 + c, pl.ds(start, rows), :]
+
+    gathers = [
+        TorusGather("y", "x", lambda a, b, s, r: place(b, a, s, r), 0, HALF, send_sems, recv_sems, 83),
+        TorusGather("x", "y", place, HALF, HALF, send_sems, recv_sems, 103),
+    ]
+
+    def share(n, j, i):
+        g = gathers[n]
+        ref = g.ref(g.order(j), shifted(g.b, (0, -1, 1, 2)[i]), None)
+        hand(123 + 16 * n + 4 * j + i, ref, ref)
+
+    def shared(n, j, i):
+        g = gathers[n]
+        a, b = g.order(j), shifted(g.b, (0, -1, 1, 2)[i])
+        xx, yy = (b, a) if n == 0 else (a, b)
+        taken(123 + 16 * n + 4 * j + i, x_all.at[xx, yy * 2 + other, pl.ds(n * HALF, HALF), :])
+
+    def weight(t):
+        return up_all[lax.div(t, 2), pl.ds(2 * lax.rem(t, 2), 2)].reshape(TOK, TOK)
+
+    def square(value, scales):
+        positive = jnp.maximum(value, 0.0) * jnp.concatenate([scales] * (TOK // HD), axis=1)
+        return (positive * positive).astype(jnp.bfloat16)
+
+    def early(blocks, first, count, step, clear, store):
+        rows = HALF * len(blocks)
+        acc = hidden_early.at[pl.ds(0, rows)]
+        if clear:
+            acc[...] = jnp.zeros_like(acc)
+
+        @pl.loop(0, count)
+        def _(i):
+            t = lax.rem(first + step * i, 8)
+            parts = [x_all[xx, t, :HALF, :] for xx in blocks]
+            part = parts[0] if len(parts) == 1 else jnp.concatenate(parts, axis=0)
+            acc[...] += jnp.dot(part, weight(t), preferred_element_type=jnp.float32)
+
+        if store:
+            for i, xx in enumerate(blocks):
+                squared[xx, :HALF, :] = square(
+                    hidden_early[i * HALF : (i + 1) * HALF, :], inverse[xx, :HALF, :]
+                )
+
+    def late(first, count, step):
+        @pl.loop(0, count)
+        def _(i):
+            t = lax.rem(first + step * i, 8)
+            rows = x_all[:, t, HALF:, :].reshape(N * HALF, TOK)
+            hidden[...] += jnp.dot(rows, weight(t), preferred_element_type=jnp.float32)
+
+    for g in gathers:
+        g.begin()
+    for n in range(2):
+        share(n, 0, 0)
     whole = stream[...]
     partial = jnp.sum(whole * whole, axis=-1, keepdims=True)
     squares[tp] = jnp.transpose(jnp.broadcast_to(partial, (TOK, HD)))[:8]
@@ -604,11 +689,16 @@
         send(squares.at[tp], squares.at[tp], send_sems.at[76 + i], recv_sems.at[76 + i], peer)
         for i, peer in enumerate(group)
     ]
-    for done in (heads, kvs, ups_across, downs_across, *columns):
+    ups.low()
+    ups.high()
+    downs.begin()
+    for g in gathers:
+        g.follow()
+    for done in (kvs, ups_across, downs_across, *columns):
         done.finish()
-    for copy in (*handed, *doc_copies, twin):
+    for copy in (*handed[:4], *heads_sent, *doc_copies, twin):
         copy.wait_send()
-    handed.clear()
+    del handed[:4]
     i = 0
     for dy in range(N):
         for cc in (c, other):
@@ -618,77 +708,24 @@
     full = squares[0]
     for t in range(1, 8):
         full = full + squares[t]
-    full = jnp.transpose(jnp.broadcast_to(full[:1], (HD, TOK)))
-    inverse = lax.rsqrt(full[:, :1] / D + norm_eps)
-    x_all[x, tp] = (stream[...] * inverse * gains[tp]).astype(jnp.bfloat16)
-
-    def place(xx, yy, start, rows):
-        return x_all.at[xx, yy * 2 + c, pl.ds(start, rows), :]
-
-    gathers = [
-        TorusGather("y", "x", lambda a, b, s, r: place(b, a, s, r), 0, HALF, send_sems, recv_sems, 83),
-        TorusGather("x", "y", place, HALF, HALF, send_sems, recv_sems, 103),
-    ]
-
-    def share(n, j, i):
-        g = gathers[n]
-        ref = g.ref(g.order(j), shifted(g.b, (0, -1, 1, 2)[i]), None)
-        hand(123 + 16 * n + 4 * j + i, ref, ref)
-
-    def shared(n, j, i):
-        g = gathers[n]
-        a, b = g.order(j), shifted(g.b, (0, -1, 1, 2)[i])
-        xx, yy = (b, a) if n == 0 else (a, b)
-        taken(123 + 16 * n + 4 * j + i, x_all.at[xx, yy * 2 + other, pl.ds(n * HALF, HALF), :])
-
-    def weight(t):
-        return up_all[lax.div(t, 2), pl.ds(2 * lax.rem(t, 2), 2)].reshape(TOK, TOK)
-
-    def square(value):
-        positive = jnp.maximum(value, 0.0)
-        return (positive * positive).astype(jnp.bfloat16)
-
-    def early(blocks, first, count, step, clear, store):
-        rows = HALF * len(blocks)
-        acc = hidden_early.at[pl.ds(0, rows)]
-        if clear:
-            acc[...] = jnp.zeros_like(acc)
-
-        @pl.loop(0, count)
-        def _(i):
-            t = lax.rem(first + step * i, 8)
-            parts = [x_all[xx, t, :HALF, :] for xx in blocks]
-            part = parts[0] if len(parts) == 1 else jnp.concatenate(parts, axis=0)
-            acc[...] += jnp.dot(part, weight(t), preferred_element_type=jnp.float32)
-
-        if store:
-            for i, xx in enumerate(blocks):
-                squared[xx, :HALF, :] = square(hidden_early[i * HALF : (i + 1) * HALF, :])
-
-    def late(first, count, step):
-        @pl.loop(0, count)
-        def _(i):
-            t = lax.rem(first + step * i, 8)
-            rows = x_all[:, t, HALF:, :].reshape(N * HALF, TOK)
-            hidden[...] += jnp.dot(rows, weight(t), preferred_element_type=jnp.float32)
-
-    for g in gathers:
-        g.begin()
-    for n in range(2):
-        share(n, 0, 0)
-    ups.low()
-    ups.high()
-    downs.begin()
-    for g in gathers:
-        g.follow()
+    totals[x] = full
     hidden[...] = jnp.zeros_like(hidden)
     for n, g in enumerate(gathers):
         g.near()
         share(n, 1, 0)
         share(n, 2, 0)
+    square_copies += [
+        send(totals.at[x], totals.at[x], send_sems.at[210 + dx], recv_sems.at[210 + dx], {"x": shifted(x, dx)})
+        for dx in range(1, N)
+    ]
     for n, g in enumerate(gathers):
         g.far()
         share(n, 3, 0)
+    for dx in range(1, N):
+        arrived(totals.at[shifted(x, -dx)], send_sems.at[210 + dx], recv_sems.at[210 + dx], {"x": x})
+    for xx in range(N):
+        full = jnp.transpose(jnp.broadcast_to(totals[xx, :1, :], (HD, TOK)))
+        inverse[xx] = lax.rsqrt(full / D + norm_eps)
     ups.far()
     for n in range(2):
         for j in range(N):
@@ -727,7 +764,7 @@
     @pl.loop(0, N)
     def _(xx):
         rows = pl.ds(pl.multiple_of(xx * HALF, HALF), HALF)
-        squared[xx, HALF:, :] = square(hidden[rows, :])
+        squared[xx, HALF:, :] = square(hidden[rows, :], inverse[xx, HALF:, :])
 
     for g in gathers:
         g.finish()
@@ -857,7 +894,7 @@
     queries, keys, values, documents, query_gain, key_gain, residual, out_weight, norm_gain, up_weight, down_weight
 ):
     bf, f32 = jnp.bfloat16, jnp.float32
-    cosine, sine = tables(lax.axis_index(("z", "x")))
+    row_table, column_table = tables()
     return pl.pallas_call(
         layer_kernel,
         out_shape=jax.ShapeDtypeStruct((TOK, TOK), bf),
@@ -874,13 +911,17 @@
             pltpu.VMEM((N, TOK, TOK), bf),
             pltpu.VMEM((8, 8, TOK), f32),
             pltpu.VMEM((TOK, TOK), f32),
+            pltpu.VMEM((N, 8, TOK), f32),
+            pltpu.VMEM((N, TOK, HD), f32),
+            pltpu.VMEM((2, TOK // GRID_W, HD), f32),
+            pltpu.VMEM((2, GRID_W, HD), f32),
             pltpu.VMEM((16, 1, TOK), jnp.int32),
             pltpu.VMEM((TOK, HD), jnp.int32),
             pltpu.VMEM((1, HD), f32),
             pltpu.VMEM((1, HD), f32),
             pltpu.VMEM((8, 1, TOK), f32),
-            pltpu.SemaphoreType.DMA((211,)),
-            pltpu.SemaphoreType.DMA((211,)),
+            pltpu.SemaphoreType.DMA((216,)),
+            pltpu.SemaphoreType.DMA((216,)),
             pltpu.SemaphoreType.DMA((13,)),
             pltpu.SemaphoreType.REGULAR,
         ],
@@ -890,7 +931,7 @@
         name="layer",
     )(
         queries, keys, values, documents.reshape(1, TOK), query_gain.reshape(1, HD), key_gain.reshape(1, HD),
-        cosine, sine, out_weight, residual, norm_gain.reshape(8, 1, TOK), up_weight, down_weight,
+        row_table, column_table, out_weight, residual, norm_gain.reshape(8, 1, TOK), up_weight, down_weight,
     )
 
 

time: 181 us -> 176 us (0.972)
  Pallas kernels: 177 us -> 173 us
  other arithmetic: 1.88 us -> 0 us
    pallas_call x1, Pallas kernels: 177 us -> 173 us  [body(): pl.pallas_call(layer_kernel, out_shape=jax.ShapeDtypeStruct((TOK, TOK), b...]
    mul x1 -> x0, other arithmetic: 1.85 us -> none  [tables(): return (jnp.cos(angles), jnp.sin(angles) * sign[None, :])]
where the time goes in v4:
time: 176 us; the launch traced here: 175 us
  Pallas kernels  173 us (98%)
  local copies, waits for them, and re-layouts  1.87 us (1%)
    pallas_call x1, Pallas kernels, body(): pl.pallas_call(layer_kernel, out_shape=jax.ShapeDtypeStruct((TOK, TOK), b...  173 us

profile of v4, /device:TPU:0, one launch (start us, length us, event | category | flops | bytes accessed | tf_op | source)
XLA Modules:
  0.0 174.7 jit_solution(11865640597290952418)
XLA Ops:
  0.0 172.9 %layer.1 = bf16[512,512]{1,0:T(8,128)(2,1)} custom-call(bf16[512,256]{1,0:T(8,128)(2,1)} %queries.1, bf16[512,128]{1,0:T(8,128)(2,1)} %keys.1, bf16[512,128]{1,0:T(8,128)(2,1)} %values.1, s32[1,512]{1,0:T(1,128)} %bitcast.5, f32[1,128]{1,0:T(1,128)} %bitcast.6, f32[1,128]{1,0:T(1,128)} %bitcast.7, f32[2,128,128]{2,1,0:T(8,128)} %constant.4.clone.row_table, ...), custom_call_target="tpu_custom_call" | custom-call | tf_op jit(solution)/shard_map/layer/pallas_call | solution.py:898
  172.9 1.9 %copy.15 = bf16[512,512]{1,0:T(8,128)(2,1)} copy(bf16[512,512]{1,0:T(8,128)(2,1)} %layer.1) | data formatting | bytes 1048576
